TPU v7x, 128 devices: a whole 4x4x4 slice. The times are simulated.
128 devices in a mesh: rep: 16 (over z, x), fs: 4 (over y), tp: 2 (over core).
Axes of the slice: x: 4, y: 4, z: 4, core: 2. Of those that a mesh axis runs over, the one named last changes fastest.
Arguments:
- inputs: bfloat16 [16384, 2048], P(('rep', 'fs', 'tp')), may hold values from -6 to 6
- out_grad: bfloat16 [16384, 2048], P(('rep', 'fs', 'tp')), may hold values from -24 to 24
- pre_act: bfloat16 [16384, 8192], P('rep', ('fs', 'tp')), may hold values from -6 to 6
- w_up: bfloat16 [2048, 8192], P('rep', ('fs', 'tp')), may hold values from -0.125 to 0.125
- w_down_t: bfloat16 [2048, 8192], P('rep', ('fs', 'tp')), may hold values from -0.0625 to 0.0625
Outputs:
- grad_in: bfloat16 [16384, 2048], P(('rep', 'fs', 'tp'))
- grad_up: float32 [2048, 8192], P('rep', ('fs', 'tp'))
- grad_down_t: float32 [2048, 8192], P('rep', ('fs', 'tp'))
All inputs are finite; a program needn't handle non-finite values.
Results may differ from a plain program's by a relative error of at most 0.014.
Values may be sent and summed in bfloat16 or wider, within the bound.
A program may use at most 128 MiB of HBM per device.

v0:
```python
import jax
import jax.numpy as jnp
from jax import lax
from jax.sharding import PartitionSpec as P


def side_by_side(arrays, axis, dim, along):
    widths = [a.shape[along] for a in arrays]
    both = jnp.concatenate(arrays, axis=along)
    out = lax.all_gather(both, axis, axis=dim, tiled=True)
    return tuple(jnp.split(out, [sum(widths[:k]) for k in range(1, len(widths))], axis=along))


def cut_along(shard, dim, length):
    shape = shard.shape
    tiles = shard.reshape(*shape[:dim], length, shape[dim] // length, *shape[dim + 1 :])
    return jnp.moveaxis(tiles, dim, 0)


def sent_and_summed(shard, axis, dim):
    tiles = cut_along(shard, dim, lax.axis_size(axis))
    arrived = lax.all_to_all(tiles, axis, split_axis=0, concat_axis=0, tiled=True)
    return arrived.astype(jnp.float32).sum(axis=0)


def on_device(inputs, out_grad, pre_act, w_up, w_down_t):
    input_rows, grad_rows = side_by_side((inputs, out_grad), ("fs", "tp"), 0, 1)
    row_count, col_count = pre_act.shape
    pre_float = pre_act.astype(jnp.float32)
    linear = jnp.maximum(pre_float, 0.0)
    squared = (linear * linear).astype(jnp.bfloat16)
    grad_squared = jnp.dot(
        grad_rows,
        lax.all_gather(w_down_t, "rep", axis=0, tiled=True),
        preferred_element_type=jnp.float32,
    )
    grad_pre = (grad_squared * 2.0 * linear).astype(jnp.bfloat16)
    partial_terms = lax.dot_general(
        grad_pre,
        lax.all_gather(w_up, "rep", axis=0, tiled=True),
        (((1,), (1,)), ((), ())),
        preferred_element_type=jnp.float32,
    ).astype(jnp.bfloat16)
    grad_in = sent_and_summed(
        partial_terms.astype(jnp.float32).astype(jnp.bfloat16), ("fs", "tp"), 0
    ).astype(jnp.bfloat16)
    total_tokens = row_count * lax.axis_size("rep")
    factor = float(total_tokens) ** (-0.5)
    down_part = lax.dot_general(
        grad_rows, squared, (((0,), (0,)), ((), ())), preferred_element_type=jnp.float32
    )
    up_part = lax.dot_general(
        input_rows, grad_pre, (((0,), (0,)), ((), ())), preferred_element_type=jnp.float32
    )
    stacked = lax.psum_scatter(
        (jnp.concatenate([down_part, up_part], axis=1) * factor).astype(jnp.bfloat16),
        "rep",
        scatter_dimension=0,
        tiled=True,
    ).astype(jnp.float32)
    grad_down_t = stacked[:, :col_count]
    grad_up = stacked[:, col_count:]
    return (grad_in, grad_up, grad_down_t)


def solution(mesh):
    in_specs = (
        P(("rep", "fs", "tp"), None),
        P(("rep", "fs", "tp"), None),
        P("rep", ("fs", "tp")),
        P("rep", ("fs", "tp")),
        P("rep", ("fs", "tp")),
    )
    out_specs = (P(("rep", "fs", "tp"), None), P("rep", ("fs", "tp")), P("rep", ("fs", "tp")))
    return jax.shard_map(
        on_device, mesh=mesh, in_specs=in_specs, out_specs=out_specs, check_vma=False
    )
```

profile of v0, /device:TPU:1, one launch (start us, length us, event | category | flops | bytes accessed | tf_op | source)
XLA Modules:
  0.0 267.0 jit_solution(14350902395174839867)
XLA Ops:
  7.2 0.0 all-gather.4.cloned.1.call-start
  7.2 2.4 pad_maximum_fusion
  9.6 0.0 all-gather.4.cloned.1.call-update
  9.6 0.0 all-gather.6.cloned.1.call-start
  9.6 0.7 all-gather.6.cloned.1.call-update
  10.3 0.0 all-gather.8.cloned.1.call-start
  10.4 0.7 all-gather.8.cloned.1.call-update
  11.1 0.0 copy-start.1
  11.1 0.0 reduce-scatter.4.cloned.1.call-start
  11.1 51.9 %all-gather.4.cloned.1.call-done = bf16[1024,4096]{1,0:T(8,128)(2,1)} async-done(((bf16[128,4096]{1,0:T(8,128)(2,1)}), bf16[1024,4096]{1,0:T(8,128)(2,1)}) %all-gather.4.cloned.1.call-update) | async-done | bytes 8388624 | tf_op jit(solution)/shard_map/all_gather | solution.py:10
  63.0 10.7 %fusion.3 = f32[2048,1024]{0,1:T(8,128)} fusion(bf16[1024,4096]{1,0:T(8,128)(2,1)} %all-gather.4.cloned.1.call-done, bf16[1024,1024]{1,0:T(8,128)(2,1)} %param.7), kind=kOutput, calls=%fused_computation.8 | convolution fusion | flops 4299161600 | bytes 14680064 | tf_op jit(solution)/shard_map/dot_general | solution.py:49
  73.7 42.6 %all-gather.6.cloned.1.call-done = bf16[2048,1024]{1,0:T(8,128)(2,1)} async-done(((bf16[128,1024]{1,0:T(8,128)(2,1)}), bf16[2048,1024]{1,0:T(8,128)(2,1)}) %all-gather.6.cloned.1.call-update) | async-done | bytes 4194320 | tf_op jit(solution)/shard_map/all_gather | solution.py:34
  116.3 0.0 copy-done.1
  116.3 0.0 copy-start
  116.3 0.0 slice-start
  116.3 8.1 %multiply_convert_fusion.1 = bf16[1024,1024]{1,0:T(8,128)(2,1)S(1)} fusion(bf16[1024,1024]{1,0:T(8,128)(2,1)S(1)} %copy-done.1, bf16[2048,1024]{1,0:T(8,128)(2,1)} %all-gather.6.cloned.1.call-done, bf16[1024,4096]{1,0:T(8,128)(2,1)} %all-gather.4.cloned.1.call-done), kind=kOutput, calls=%fused_computation.5 | convolution fusion | flops 4300210176 | bytes 12582912 | tf_op jit(solution)/shard_map/dot_general | solution.py:32
  124.4 0.0 copy-done
  124.4 0.0 copy-start.2
  124.4 0.0 slice-start.1
  124.4 4.9 %fusion.1 = f32[2048,1024]{0,1:T(8,128)S(1)} fusion(bf16[1024,1024]{1,0:T(8,128)(2,1)S(1)} %multiply_convert_fusion.1, bf16[1024,4096]{1,0:T(8,128)(2,1)S(1)} %copy-done), kind=kOutput, calls=%fused_computation.2 | convolution fusion | flops 4294967296 | bytes 14680064 | tf_op jit(solution)/shard_map/dot_general | solution.py:52
  129.4 0.0 copy-done.2
  129.4 0.0 slice-done
  129.4 0.0 slice-done.1
  129.4 4.8 %fusion = bf16[2048,2048]{0,1:T(8,128)(2,1)} fusion(f32[2048,1024]{0,1:T(8,128)S(1)} %fusion.1, f32[2048,1024]{0,1:T(8,128)S(1)} %bitcast.7), kind=kLoop, calls=%fused_computation.1 | loop fusion | flops 12582912 | bytes 25165824 | tf_op jit(solution)/shard_map/convert_element_type | solution.py:56
  134.2 12.3 %copy.12 = bf16[2048,2048]{1,0:T(8,128)(2,1)} copy(bf16[2048,2048]{0,1:T(8,128)(2,1)} %fusion) | data formatting | bytes 16777216
  146.5 0.0 copy-start.3
  146.5 0.0 reduce-scatter.4.cloned.1.call-update
  146.5 23.0 %all-gather.8.cloned.1.call-done = bf16[2048,1024]{1,0:T(8,128)(2,1)} async-done(((bf16[128,1024]{1,0:T(8,128)(2,1)}), bf16[2048,1024]{1,0:T(8,128)(2,1)}) %all-gather.8.cloned.1.call-update) | async-done | bytes 4194320 | tf_op jit(solution)/shard_map/all_gather | solution.py:40
  169.5 0.0 copy-done.3
  169.5 6.9 %convolution_convert_fusion = bf16[1024,2048]{1,0:T(8,128)(2,1)S(1)} fusion(bf16[1024,1024]{1,0:T(8,128)(2,1)S(1)} %copy-done.3, bf16[2048,1024]{1,0:T(8,128)(2,1)} %all-gather.8.cloned.1.call-done), kind=kOutput, calls=%fused_computation.7 | convolution fusion | flops 4297064448 | bytes 10485760 | tf_op jit(solution)/shard_map/dot_general | solution.py:38
  176.4 53.7 %all_to_all.5 = bf16[8,128,2048]{2,1,0:T(8,128)(2,1)} all-to-all(bf16[8,128,2048]{2,1,0:T(8,128)(2,1)S(1)} %bitcast.8), channel_id=1, replica_groups=mesh['rep'=16,'fs'=4,'tp'=2] {'fs','tp'}, dimensions={0} | all-to-all | bytes 8388608 | tf_op jit(solution)/shard_map/all_to_all | solution.py:22
  230.1 3.8 %reduce_sum.12 = bf16[128,2048]{1,0:T(8,128)(2,1)} reduce(bf16[8,128,2048]{2,1,0:T(8,128)(2,1)} %all_to_all.5, bf16[]{:T(256)} %constant.3.clone.1), dimensions={0}, to_apply=%region_0.0 | reduce | flops 1835008 | bytes 4718594 | tf_op jit(solution)/shard_map/reduce_sum | solution.py:23
  234.0 23.1 %reduce-scatter.4.cloned.1.call-done = bf16[128,2048]{1,0:T(8,128)(2,1)} async-done(((bf16[2048,2048]{1,0:T(8,128)(2,1)}), bf16[128,2048]{1,0:T(8,128)(2,1)}) %reduce-scatter.4.cloned.1.call-update) | async-done | bytes 524304
  257.1 1.3 copy.13
  258.4 0.1 fusion.11
  258.5 1.0 copy.11
  259.5 1.0 copy.10
  (1 shorter events, 0.0 us)
Async XLA Ops:
  7.2 55.9 %all-gather.4.cloned.1.call-start = ((), (), s32[]{:S(2)}) async-start(), calls=%async_computation.2 | async-start | bytes 9437184 | tf_op jit(solution)/shard_map/all_gather | solution.py:10
  9.6 106.7 %all-gather.6.cloned.1.call-start = ((), (), s32[]{:S(2)}) async-start(), calls=%async_computation.3 | async-start | bytes 4456448 | tf_op jit(solution)/shard_map/all_gather | solution.py:34
  10.3 159.2 %all-gather.8.cloned.1.call-start = ((), (), s32[]{:S(2)}) async-start(), calls=%async_computation.4 | async-start | bytes 4456448 | tf_op jit(solution)/shard_map/all_gather | solution.py:40
  11.1 105.2 %copy-start.1 = (bf16[1024,1024]{1,0:T(8,128)(2,1)S(1)}, bf16[1024,1024]{1,0:T(8,128)(2,1)}, u32[]{:S(2)}) copy-start(bf16[1024,1024]{1,0:T(8,128)(2,1)} %param.7) | copy-start | bytes 6291460
  11.1 246.0 %reduce-scatter.4.cloned.1.call-start = ((), (), s32[]{:S(2)}) async-start(), calls=%async_computation.5 | async-start | bytes 8912896
  116.3 8.1 %copy-start = (bf16[1024,4096]{1,0:T(8,128)(2,1)S(1)}, bf16[1024,4096]{1,0:T(8,128)(2,1)}, u32[]{:S(2)}) copy-start(bf16[1024,4096]{1,0:T(8,128)(2,1)} %all-gather.4.cloned.1.call-done) | copy-start | bytes 25165828
  116.3 13.1 %slice-start = ((s8[8388608]{0:T(1024)(128)(4,1)}), s8[4194304]{0:T(1024)(128)(4,1)S(1)}, s32[]{:S(2)}) async-start(s8[8388608]{0:T(1024)(128)(4,1)} %bitcast.6), calls=%async_computation.6 | async-start | bytes 8388608
  124.4 5.0 %copy-start.2 = (bf16[1024,1024]{1,0:T(8,128)(2,1)}, bf16[1024,1024]{1,0:T(8,128)(2,1)S(1)}, u32[]{:S(2)}) copy-start(bf16[1024,1024]{1,0:T(8,128)(2,1)S(1)} %multiply_convert_fusion.1) | copy-start | bytes 6291460
  124.4 5.0 %slice-start.1 = ((s8[8388608]{0:T(1024)(128)(4,1)}), s8[4194304]{0:T(1024)(128)(4,1)S(1)}, s32[]{:S(2)}) async-start(s8[8388608]{0:T(1024)(128)(4,1)} %bitcast.6), calls=%async_computation.7 | async-start | bytes 8388608
  146.5 23.0 %copy-start.3 = (bf16[1024,1024]{1,0:T(8,128)(2,1)S(1)}, bf16[1024,1024]{1,0:T(8,128)(2,1)}, u32[]{:S(2)}) copy-start(bf16[1024,1024]{1,0:T(8,128)(2,1)} %copy-done.2) | copy-start | bytes 6291460
Sparse Core Ops, SparseCore 0:
  9.7 53.2 all-gather.3
  65.2 51.0 all-gather.5
  118.4 51.0 all-gather.7
  172.8 84.3 reduce-scatter.3
where the time goes:
time: 268 us; the launch traced here: 267 us
  waiting for transfers between devices  142 us (53%)
  blocking collectives  53.7 us (20%)
  matrix products  30.6 us (11%)
  local copies, waits for them, and re-layouts  15.7 us (6%)
  between operations  13.9 us (5%)
  other arithmetic  11 us (4%)
    all_to_all x1, blocking collectives, sent_and_summed(): lax.all_to_all(tiles, axis, split_axis=0, concat_axis=0, tiled=True)  53.7 us
    all_gather x1, waiting for transfers between devices, side_by_side(): out = lax.all_gather(both, axis, axis=dim, tiled=True)  51.9 us
    all_gather x1, waiting for transfers between devices, on_device(): lax.all_gather(w_down_t, 'rep', axis=0, tiled=True)  42.6 us
    unnamed x5, waiting for transfers between devices  24.5 us
    all_gather x1, waiting for transfers between devices, on_device(): lax.all_gather(w_up, 'rep', axis=0, tiled=True)  23 us
    unnamed x16, local copies, waits for them, and re-layouts  15.6 us
    dot_general x1, matrix products, on_device(): lax.dot_general(grad_rows, squared, (((0,), (0,)), ((), ())), preferred_e...  10.7 us
    dot_general x1, matrix products, on_device(): jnp.dot(grad_rows, lax.all_gather(w_down_t, 'rep', axis=0, tiled=True), p...  8.09 us
  transfers between devices with their start and end apart: 4, of which 4 were waited for; matrix products, arithmetic and copies ran while one was open for 19% of the time, Pallas kernels for 0%

commit v1 on v0

v1 whole, which is shorter than its diff:
```python
import jax
import jax.numpy as jnp
from jax import lax
from jax.experimental import pallas as pl
from jax.experimental.pallas import tpu as pltpu
from jax.sharding import PartitionSpec as P

MESH = pl.DeviceIdType.MESH
BF16, F32 = jnp.bfloat16, jnp.float32
STEP = {"zp": (1, 0), "zm": (-1, 0), "xp": (0, 1), "xm": (0, -1)}
PLUS = ((0, 2), (1, 3))
TURN = (1, -1)
SEMS = 160


def kernel(
    inp, og, pre_in, wu_in, wd_in, gi_out, gu_out, gd_out,
    tok_g, tok_x, w_d, w_u, pre, sq, gp, turned, part_d, part_u, part_i,
    fwd1, lft1, rgt1, sum1, fwd2, lft2, rgt2,
    pair_in, hop_f, hop_l, hop_r, res_i, res_w, send_sem, recv_sem, local_sem,
):
    rep, fs, tp = lax.axis_index("rep"), lax.axis_index("fs"), lax.axis_index("tp")
    z, x = lax.div(rep, 4), lax.rem(rep, 4)
    tokens, weights, parts = (tok_g, tok_x), (w_d, w_u), (part_d, part_u)
    factor = 1.0 / 128.0

    def ring(v, d):
        return lax.rem(v + d % 4, 4)

    target = {
        "zp": {"rep": ring(z, 1) * 4 + x},
        "zm": {"rep": ring(z, -1) * 4 + x},
        "xp": {"rep": z * 4 + ring(x, 1)},
        "xm": {"rep": z * 4 + ring(x, -1)},
        "yp": {"fs": ring(fs, 1)},
        "ym": {"fs": ring(fs, -1)},
        "co": {"tp": 1 - tp},
    }
    ids, started = {}, []

    def remote(to, src, dst, key):
        n = ids.setdefault(key, len(ids))
        return pltpu.make_async_remote_copy(
            src_ref=src, dst_ref=dst, send_sem=send_sem.at[n], recv_sem=recv_sem.at[n],
            device_id=target[to], device_id_type=MESH,
        )

    def send(to, src, dst, key):
        copy = remote(to, src, dst, key)
        copy.start()
        started.append(copy)

    def got(dst, key):
        remote("co", dst, dst, key).wait_recv()

    def rows(start, size):
        return pl.ds(pl.multiple_of(start, size), size)

    def add(dst, *srcs, size=32, scale=None):
        def one(i, carry):
            r = rows(i * size, size)
            total = srcs[0][r, :].astype(F32)
            for src in srcs[1:]:
                total = total + src[r, :].astype(F32)
            if scale is not None:
                total = total * scale
            dst[r, :] = total.astype(dst.dtype)
            return carry

        lax.fori_loop(0, dst.shape[0] // size, one, 0)

    def tok(a, df, mine, h):
        core = tp if mine else 1 - tp
        return tokens[a].at[rows((ring(fs, df) * 2 + core) * 128 + h * 64, 64), :]

    def tok_y(a, df, h, s):
        p = tok(a, df, True, h)
        send("yp" if s > 0 else "ym", p, p, ("t", a, (df - s) % 4, True, h))

    def tok_co(a, df, h):
        p = tok(a, df, True, h)
        send("co", p, p, ("t", a, df % 4, False, h))

    def tok_got(a, df, mine, h):
        got(tok(a, df, mine, h), ("t", a, df % 4, mine, h))

    def tok_own(a):
        tok_y(a, 0, 0, 1)
        tok_y(a, 0, 1, -1)
        tok_y(a, 0, 1, 1)
        tok_y(a, 0, 0, -1)
        tok_co(a, 0, 0)
        tok_co(a, 0, 1)

    def tok_first(a):
        for df, h in ((-1, 0), (1, 1)):
            tok_got(a, df, True, h)
            tok_y(a, df, h, -df)
            tok_co(a, df, h)

    def tok_second(a):
        for df, h in ((-1, 1), (1, 0)):
            tok_got(a, df, True, h)
            tok_co(a, df, h)

    def tok_third(a):
        for h in (0, 1):
            tok_got(a, 2, True, h)
            tok_co(a, 2, h)

    def tok_partner(a):
        for df in (0, -1, 1, 2):
            for h in (0, 1):
                tok_got(a, df, False, h)

    def chunk(dz, dx):
        return (ring(z, dz) * 4 + ring(x, dx)) * 128

    def offs(half, d1, d2):
        return (d1, d2) if half == 0 else (d2, d1)

    def way(half, second, s):
        return ("zx"[half ^ second]) + ("p" if s > 0 else "m")

    def w_piece(w, half, d1, d2):
        dz, dx = offs(half, d1, d2)
        return weights[w].at[rows(chunk(dz, dx) + half * 64, 64), :]

    def w_send(w, half, d1, d2, second, s):
        p = w_piece(w, half, d1, d2)
        e1, e2 = (0, s) if second else (s, 0)
        send(way(half, second, s), p, p, ("w", w, half, (d1 - e1) % 4, (d2 - e2) % 4))

    def w_got(w, half, d1, d2):
        got(w_piece(w, half, d1, d2), ("w", w, half, d1 % 4, d2 % 4))

    def w_own(w):
        for second in (0, 1):
            for half in (0, 1):
                for s in (1, -1):
                    w_send(w, half, 0, 0, second, s)

    def w_first(w):
        for s in (TURN[w], -TURN[w]):
            for half in (0, 1):
                w_got(w, half, -s, 0)
                if s == TURN[w]:
                    w_send(w, half, -s, 0, 0, s)
                for e in (1, -1):
                    w_send(w, half, -s, 0, 1, e)

    def w_second(w):
        for half in (0, 1):
            w_got(w, half, 2, 0)
            for e in (1, -1):
                w_send(w, half, 2, 0, 1, e)

    def w_third(w, d1s):
        for d1 in d1s:
            for half in (0, 1):
                for s in (1, -1):
                    w_got(w, half, d1, -s)
                    if s == (1 if d1 in PLUS[w] else -1):
                        w_send(w, half, d1, -s, 1, s)

    def w_last(w):
        for d1 in (0, 1, 3, 2):
            for half in (0, 1):
                w_got(w, half, d1, 2)

    def unit(w, half, da, db):
        dz, dx = (db, da) if half == 0 else (da, db)
        return parts[w].at[rows(chunk(dz, dx), 128), half * 512 : half * 512 + 512]

    def rs_way(half, second, s):
        return way(1 - half, second, s)

    def sign(w, db):
        return 1 if db % 4 in PLUS[w] else -1

    def end1(s):
        return (lft1, "l1") if s > 0 else (rgt1, "r1")

    def end2(s):
        return (lft2, "l2") if s > 0 else (rgt2, "r2")

    def rs_far(w, half, db):
        db = db % 4
        send(rs_way(half, 0, sign(w, db)), unit(w, half, 2, db), fwd1.at[w, half, db], ("f1", w, half, db))

    def rs_near(w, half, db):
        db, s = db % 4, -sign(w, db)
        buf, name = end1(s)
        send(rs_way(half, 0, s), unit(w, half, s, db), buf.at[w, half, db], (name, w, half, db))

    def rs_relay(w, half, db):
        db, s = db % 4, sign(w, db)
        got(fwd1.at[w, half, db], ("f1", w, half, db))
        mine = unit(w, half, s, db)
        add(mine, mine, fwd1.at[w, half, db])
        buf, name = end1(s)
        send(rs_way(half, 0, s), mine, buf.at[w, half, db], (name, w, half, db))

    def rs_mid(w, half, db):
        db, s = db % 4, TURN[w]
        for e in (1, -1):
            buf, name = end1(e)
            got(buf.at[w, half, db], (name, w, half, db))
        terms = [unit(w, half, 0, db), lft1.at[w, half, db], rgt1.at[w, half, db]]
        mine = sum1.at[w, half, db]
        if db == 2:
            add(mine, *terms)
            send(rs_way(half, 1, s), mine, fwd2.at[w, half], ("f2", w, half))
        elif db == -s % 4:
            add(mine, *terms)
            buf, name = end2(-s)
            send(rs_way(half, 1, -s), mine, buf.at[w, half], (name, w, half))
        elif db == s % 4:
            got(fwd2.at[w, half], ("f2", w, half))
            add(mine, *terms, fwd2.at[w, half])
            buf, name = end2(s)
            send(rs_way(half, 1, s), mine, buf.at[w, half], (name, w, half))
        else:
            for e in (1, -1):
                buf, name = end2(e)
                got(buf.at[w, half], (name, w, half))
            add(
                res_w.at[w, :, half * 512 : half * 512 + 512],
                *terms, lft2.at[w, half], rgt2.at[w, half], scale=factor,
            )

    def rs_start(w, dz):
        if dz == 2:
            rs_far(w, 0, 2)
            for db in (2, 1, 3, 0):
                rs_far(w, 1, db)
            rs_near(w, 0, 2)
        else:
            rs_far(w, 0, dz)
            rs_near(w, 0, dz)
            if dz != 0:
                for db in (2, 1, 3, 0):
                    if (1 if dz == 1 else -1) == -sign(w, db):
                        rs_near(w, 1, db)

    def block(df, mine):
        core = tp if mine else 1 - tp
        return (ring(fs, df) * 2 + core) * 128

    def gi_rows(df, h):
        return part_i.at[rows(block(df, True) + h * 64, 64), :]

    def gi_pair():
        for df in (2, 1, 3, 0):
            src = part_i.at[rows(block(df, False), 128), :]
            send("co", src, pair_in.at[df], ("pi", df))

    def gi_sum(df):
        got(pair_in.at[df], ("pi", df))
        mine = part_i.at[rows(block(df, True), 128), :]
        if df != 0:
            add(mine, mine, pair_in.at[df], size=16)

    def gi_far():
        gi_sum(2)
        send("yp", gi_rows(2, 0), hop_f.at[0], ("gf", 0))
        send("ym", gi_rows(2, 1), hop_f.at[1], ("gf", 1))
        gi_sum(1)
        send("yp", gi_rows(1, 1), hop_l.at[1], ("gl", 1))
        gi_sum(3)
        send("ym", gi_rows(3, 0), hop_r.at[0], ("gr", 0))
        gi_sum(0)

    def gi_relay():
        got(hop_f.at[0], ("gf", 0))
        add(gi_rows(1, 0), gi_rows(1, 0), hop_f.at[0], size=16)
        send("yp", gi_rows(1, 0), hop_l.at[0], ("gl", 0))
        got(hop_f.at[1], ("gf", 1))
        add(gi_rows(3, 1), gi_rows(3, 1), hop_f.at[1], size=16)
        send("ym", gi_rows(3, 1), hop_r.at[1], ("gr", 1))

    def gi_end():
        for h in (0, 1):
            got(hop_l.at[h], ("gl", h))
            got(hop_r.at[h], ("gr", h))
            add(
                res_i.at[pl.ds(h * 64, 64), :],
                gi_rows(0, h), pair_in.at[0, pl.ds(h * 64, 64), :], hop_l.at[h], hop_r.at[h], size=16,
            )

    def squares():
        def one(i, carry):
            r = rows(i * 32, 32)
            linear = jnp.maximum(pre[r, :].astype(F32), 0.0)
            sq[r, :] = (linear * linear).astype(BF16)
            return carry

        lax.fori_loop(0, 32, one, 0)

    def grad_tile(w, dz):
        right = (sq, gp)[w]
        start = ring(z, dz) * 512
        turned[...] = tokens[w][:, rows(start, 512)].T

        def one(j, carry):
            c = rows(j * 512, 512)
            parts[w][rows(start, 512), c] = jnp.dot(
                turned[...], right[:, c], preferred_element_type=F32
            ).astype(BF16)
            return carry

        lax.fori_loop(0, 2, one, 0)

    def pre_tile(i):
        def one(j, carry):
            r, c = rows(i * 512, 512), rows(j * 256, 256)
            acc = jnp.dot(tok_g[r, :], w_d[:, c], preferred_element_type=F32)
            linear = jnp.maximum(pre[r, c].astype(F32), 0.0)
            gp[r, c] = (acc * 2.0 * linear).astype(BF16)
            return carry

        lax.fori_loop(0, 4, one, 0)

    def term_tile(i):
        def one(j, carry):
            r, c = rows(i * 512, 512), rows(j * 512, 512)
            part_i[r, c] = lax.dot_general(
                gp[r, :], w_u[c, :], (((1,), (1,)), ((), ())), preferred_element_type=F32
            ).astype(BF16)
            return carry

        lax.fori_loop(0, 4, one, 0)

    own = rows((fs * 2 + tp) * 128, 128)
    mine = rows(rep * 128, 128)
    local = [
        pltpu.make_async_copy(src, dst, local_sem.at[n])
        for n, (src, dst) in enumerate(
            (
                (wd_in, w_d.at[mine, :]),
                (og, tok_g.at[own, :]),
                (wu_in, w_u.at[mine, :]),
                (inp, tok_x.at[own, :]),
                (pre_in, pre),
            )
        )
    ]
    for copy in local:
        copy.start()
    barrier = pltpu.get_barrier_semaphore()
    for to in target.values():
        pl.semaphore_signal(barrier, inc=1, device_id=to, device_id_type=MESH)
    pl.semaphore_wait(barrier, len(target))

    local[0].wait()
    w_own(0)
    local[1].wait()
    tok_own(0)
    local[2].wait()
    local[3].wait()
    local[4].wait()
    squares()
    w_first(0)
    tok_first(0)
    tok_own(1)
    w_third(0, (0,))
    w_second(0)
    w_own(1)
    tok_second(0)
    w_third(0, (1, 3))
    w_first(1)
    tok_third(0)
    tok_partner(0)
    grad_tile(0, 2)
    rs_start(0, 2)
    w_third(0, (2,))
    grad_tile(0, 1)
    rs_start(0, 1)
    w_second(1)
    tok_first(1)
    grad_tile(0, 3)
    rs_start(0, 3)
    w_third(1, (0,))
    grad_tile(0, 0)
    rs_start(0, 0)
    w_last(0)
    pre_tile(0)
    w_third(1, (1, 3))
    tok_second(1)
    pre_tile(1)
    w_third(1, (2,))
    tok_third(1)
    tok_partner(1)
    grad_tile(1, 2)
    rs_start(1, 2)
    grad_tile(1, 1)
    rs_start(1, 1)
    grad_tile(1, 3)
    rs_start(1, 3)
    grad_tile(1, 0)
    rs_start(1, 0)
    w_last(1)
    term_tile(0)
    for db in (2, 1):
        for half in (0, 1):
            rs_relay(0, half, db)
    term_tile(1)
    gi_pair()
    for db in (3, 0):
        for half in (0, 1):
            rs_relay(0, half, db)
    gi_far()
    for w in (0, 1):
        order = (2, -TURN[w], TURN[w], 0)
        if w == 0:
            for db in (2, 1, 3, 0):
                for half in (0, 1):
                    rs_mid(0, half, order[0]) if db == 2 else None
                    rs_relay(1, half, db)
            gi_relay()
            for db in order[1:]:
                for half in (0, 1):
                    rs_mid(0, half, db)
        else:
            gi_end()
            for db in order:
                for half in (0, 1):
                    rs_mid(1, half, db)
    outs = [
        pltpu.make_async_copy(src, dst, local_sem.at[n])
        for n, (src, dst) in enumerate(((res_i, gi_out), (res_w.at[1], gu_out), (res_w.at[0], gd_out)))
    ]
    for copy in outs:
        copy.start()
    for copy in started:
        copy.wait_send()
    for copy in outs:
        copy.wait()


def on_device(inputs, out_grad, pre_act, w_up, w_down_t):
    anywhere = pl.BlockSpec(memory_space=pl.ANY)

    def vm(*shape, kind=BF16):
        return pltpu.VMEM(shape, kind)

    return pl.pallas_call(
        kernel,
        out_shape=(
            jax.ShapeDtypeStruct((128, 2048), BF16),
            jax.ShapeDtypeStruct((128, 1024), F32),
            jax.ShapeDtypeStruct((128, 1024), F32),
        ),
        in_specs=[anywhere] * 5,
        out_specs=(anywhere,) * 3,
        scratch_shapes=[
            vm(1024, 2048), vm(1024, 2048), vm(2048, 1024), vm(2048, 1024),
            vm(1024, 1024), vm(1024, 1024), vm(1024, 1024), vm(512, 1024),
            vm(2048, 1024), vm(2048, 1024), vm(1024, 2048),
            vm(2, 2, 4, 128, 512), vm(2, 2, 4, 128, 512), vm(2, 2, 4, 128, 512), vm(2, 2, 4, 128, 512),
            vm(2, 2, 128, 512), vm(2, 2, 128, 512), vm(2, 2, 128, 512),
            vm(4, 128, 2048), vm(2, 64, 2048), vm(2, 64, 2048), vm(2, 64, 2048),
            vm(128, 2048), vm(2, 128, 1024, kind=F32),
            pltpu.SemaphoreType.DMA((SEMS,)), pltpu.SemaphoreType.DMA((SEMS,)), pltpu.SemaphoreType.DMA((8,)),
        ],
        compiler_params=pltpu.CompilerParams(
            collective_id=0, has_side_effects=True, vmem_limit_bytes=67_000_000
        ),
        name="backward",
    )(inputs, out_grad, pre_act, w_up, w_down_t)


def solution(mesh):
    rows_all = P(("rep", "fs", "tp"), None)
    tiles = P("rep", ("fs", "tp"))
    return jax.shard_map(
        on_device,
        mesh=mesh,
        in_specs=(rows_all, rows_all, tiles, tiles, tiles),
        out_specs=(rows_all, tiles, tiles),
        check_vma=False,
    )
```

time: 268 us -> 111 us (0.41)
  waiting for transfers between devices: 142 us -> 0 us
  Pallas kernels: 0 us -> 104 us
  blocking collectives: 53.7 us -> 0 us
  matrix products: 30.6 us -> 0 us
  between operations: 13.9 us -> 0.65 us
  local copies, waits for them, and re-layouts: 15.7 us -> 4.62 us
  other arithmetic: 11 us -> 0 us
    all_gather x3 -> x0, waiting for transfers between devices: 117 us -> none  [the longest x1 51.9 us: side_by_side(): out = lax.all_gather(both, axis, axis=dim, tiled=True)]
    pallas_call x0 -> x1, Pallas kernels: none -> 104 us  [on_device(): pl.pallas_call(kernel, out_shape=(jax.ShapeDtypeStruct((128, 2048), BF16)...]
    all_to_all x1 -> x0, blocking collectives: 53.7 us -> none  [sent_and_summed(): lax.all_to_all(tiles, axis, split_axis=0, concat_axis=0, tiled=True)]
    dot_general x4 -> x0, matrix products: 30.6 us -> none  [the longest x1 10.7 us: on_device(): lax.dot_general(grad_rows, squared, (((0,), (0,)), ((), ())), preferred_e...]
    unnamed x5 -> x0, waiting for transfers between devices: 24.5 us -> none
    unnamed x16 -> x5, local copies, waits for them, and re-layouts: 15.6 us -> 4.62 us
    convert_element_type x1 -> x0, other arithmetic: 4.79 us -> none  [on_device(): (jnp.concatenate([down_part, up_part], axis=1) * factor).astype(jnp.bfloa...]
    reduce_sum x1 -> x0, other arithmetic: 3.85 us -> none  [sent_and_summed(): return arrived.astype(jnp.float32).sum(axis=0)]
  transfers between devices with their start and end apart: 4 -> 0, of which waited for: 4 -> 0; matrix products, arithmetic and copies ran while one was open for 19% -> 0% of each run, Pallas kernels for 0% -> 0%
where the time goes in v1:
time: 111 us; the launch traced here: 109 us
  Pallas kernels  104 us (94%)
  local copies, waits for them, and re-layouts  4.62 us (4%)
    pallas_call x1, Pallas kernels, on_device(): pl.pallas_call(kernel, out_shape=(jax.ShapeDtypeStruct((128, 2048), BF16)...  104 us
    unnamed x5, local copies, waits for them, and re-layouts  4.62 us

profile of v1, /device:TPU:1, one launch (start us, length us, event | category | flops | bytes accessed | tf_op | source)
XLA Modules:
  0.0 109.4 jit_solution(15668956876497414758)
XLA Ops:
  0.6 104.1 %backward.1 = (bf16[128,2048]{1,0:T(8,128)(2,1)}, f32[128,1024]{1,0:T(8,128)}, f32[128,1024]{1,0:T(8,128)}) custom-call(bf16[128,2048]{1,0:T(8,128)(2,1)} %inp.1, bf16[128,2048]{1,0:T(8,128)(2,1)} %og.1, bf16[1024,1024]{1,0:T(8,128)(2,1)} %pre_in.1, bf16[128,1024]{1,0:T(8,128)(2,1)} %wu_in.1, bf16[128,1024]{1,0:T(8,128)(2,1)} %wd_in.1), custom_call_target="tpu_custom_call" | custom-call | tf_op jit(solution)/shard_map/backward/pallas_call | solution.py:447
  104.7 0.0 copy-start
  104.8 1.9 %copy.11 = bf16[128,2048]{1,0:T(8,128)(2,1)} copy(bf16[128,2048]{1,0:T(8,128)(2,1)} %get-tuple-element.6) | data formatting | bytes 1048576
  106.7 1.9 %copy.12 = f32[128,1024]{1,0:T(8,128)} copy(f32[128,1024]{1,0:T(8,128)} %get-tuple-element.7) | data formatting | bytes 1048576
  108.6 0.0 copy-done
  108.6 0.8 copy.13
Async XLA Ops:
  104.7 3.8 %copy-start = (f32[128,1024]{1,0:T(8,128)S(1)}, f32[128,1024]{1,0:T(8,128)}, u32[]{:S(2)}) copy-start(f32[128,1024]{1,0:T(8,128)} %get-tuple-element.8) | copy-start | bytes 1572868

commit v2 on v1

v2 whole, which is shorter than its diff:
```python
import jax
import jax.numpy as jnp
from jax import lax
from jax.experimental import pallas as pl
from jax.experimental.pallas import tpu as pltpu
from jax.sharding import PartitionSpec as P

MESH = pl.DeviceIdType.MESH
BF16, F32 = jnp.bfloat16, jnp.float32
STEP = {"zp": (1, 0), "zm": (-1, 0), "xp": (0, 1), "xm": (0, -1)}
PLUS = ((0, 2), (1, 3))
TURN = (1, -1)
PLAN = (
    ("begin",), ("squares",), ("w_own", 1), ("tok_first", 0), ("w_first", 0, 1), ("w_first", 0, -1),
    ("w_first", 1, -1), ("tok_own", 1), ("tok_third", 0), ("w_second", 0), ("tok_second", 0), ("w_second", 1),
    ("w_third", 0, 3), ("tok_partner", 0), ("w_third", 0, 0), ("grad_tile", 0, 2), ("w_third", 0, 1),
    ("tok_first", 1), ("w_first", 1, 1), ("w_third", 1, 2), ("w_third", 0, 2), ("grad_tile", 0, 1),
    ("rs_far", 0, 2), ("grad_tile", 0, 0), ("rs_near", 0, 1), ("grad_tile", 0, 3), ("rs_far", 0, 3),
    ("w_third", 1, 0), ("w_last", 0), ("w_third", 1, 1), ("w_third", 1, 3), ("pre_tile", 1, 1),
    ("tok_second", 1), ("pre_tile", 0, 0), ("pre_tile", 0, 1), ("rs_near", 0, 0), ("tok_third", 1),
    ("rs_relay", 0, 2), ("tok_partner", 1), ("pre_tile", 1, 0), ("rs_near", 0, 2), ("rs_far", 0, 0),
    ("grad_tile", 1, 2), ("rs_far", 0, 1), ("rs_far", 1, 2), ("grad_tile", 1, 1), ("grad_tile", 1, 3),
    ("rs_relay", 0, 3), ("rs_far", 1, 1), ("rs_near", 1, 1), ("w_last", 1), ("rs_far", 1, 3),
    ("term_tile", 0, 1), ("grad_tile", 1, 0), ("term_tile", 0, 0), ("rs_near", 0, 3), ("term_tile", 1, 1),
    ("rs_near", 1, 0), ("rs_relay", 1, 2), ("rs_near", 1, 2), ("rs_far", 1, 0), ("term_tile", 1, 0),
    ("rs_mid", 0, 2), ("gi_pair",), ("rs_relay", 0, 1), ("rs_relay", 1, 3), ("rs_relay", 1, 1),
    ("rs_relay", 0, 0), ("gi_far",), ("rs_near", 1, 3), ("rs_mid", 1, 2), ("rs_mid", 0, 3), ("gi_relay",),
    ("rs_mid", 0, 1), ("rs_relay", 1, 0), ("rs_mid", 1, 3), ("rs_mid", 1, 1), ("rs_mid", 0, 0), ("gi_end",),
    ("rs_mid", 1, 0), ("finish",),
)


def kernel(
    inp, og, pre_in, wu_in, wd_in, gi_out, gu_out, gd_out,
    tok_g, tok_x, w_d, w_u, pre, sq, gp, turned, part_d, part_u, part_i,
    fwd1, lft1, rgt1, sum1, fwd2, lft2, rgt2,
    pair_in, hop_f, hop_l, hop_r, send_sem, recv_sem, local_sem,
):
    rep, fs, tp = lax.axis_index("rep"), lax.axis_index("fs"), lax.axis_index("tp")
    z, x = lax.div(rep, 4), lax.rem(rep, 4)
    tokens, weights, parts = (tok_g, tok_x), (w_d, w_u), (part_d, part_u)
    factor = 1.0 / 128.0

    def ring(v, d):
        return lax.rem(v + d % 4, 4)

    target = {
        "zp": {"rep": ring(z, 1) * 4 + x},
        "zm": {"rep": ring(z, -1) * 4 + x},
        "xp": {"rep": z * 4 + ring(x, 1)},
        "xm": {"rep": z * 4 + ring(x, -1)},
        "yp": {"fs": ring(fs, 1)},
        "ym": {"fs": ring(fs, -1)},
        "co": {"tp": 1 - tp},
    }
    groups, classes = {}, {}

    def remote(to, src, dst, group, kind):
        k = classes.setdefault(kind, len(classes))
        n = groups.setdefault(group, len(groups))
        return pltpu.make_async_remote_copy(
            src_ref=src, dst_ref=dst, send_sem=send_sem.at[k], recv_sem=recv_sem.at[n],
            device_id=target[to], device_id_type=MESH,
        )

    def send(to, src, dst, group):
        remote(to, src, dst, group, (group[0], *group[1:2])).start()

    def got(like, group):
        remote("co", like, like, group, (group[0], *group[1:2])).wait_recv()

    def sent(like, kind):
        remote("co", like, like, (), kind).wait_send()

    def rows(start, size):
        return pl.ds(pl.multiple_of(start, size), size)

    def add(dst, *srcs, size=32, scale=None):
        def one(i, carry):
            r = rows(i * size, size)
            total = srcs[0][r, :].astype(F32)
            for src in srcs[1:]:
                total = total + src[r, :].astype(F32)
            if scale is not None:
                total = total * scale
            dst[r, :] = total.astype(dst.dtype)
            return carry

        lax.fori_loop(0, dst.shape[0] // size, one, 0)

    def tok(a, df, mine, h):
        core = tp if mine else 1 - tp
        return tokens[a].at[rows((ring(fs, df) * 2 + core) * 128 + h * 64, 64), :]

    def tok_y(a, df, h, s, stage):
        p = tok(a, df, True, h)
        send("yp" if s > 0 else "ym", p, p, ("tok", a, stage))

    def tok_co(a, df, h):
        p = tok(a, df, True, h)
        send("co", p, p, ("tok", a, "partner"))

    def tok_got(a, pieces, stage):
        got(tokens[a].at[0 : 64 * pieces, :], ("tok", a, stage))

    def tok_own(a):
        tok_y(a, 0, 0, 1, 1)
        tok_y(a, 0, 1, -1, 1)
        tok_y(a, 0, 1, 1, 2)
        tok_y(a, 0, 0, -1, 2)
        tok_co(a, 0, 0)
        tok_co(a, 0, 1)

    def tok_first(a):
        tok_got(a, 2, 1)
        for df, h in ((-1, 0), (1, 1)):
            tok_y(a, df, h, -df, 3)
            tok_co(a, df, h)

    def tok_second(a):
        tok_got(a, 2, 2)
        for df, h in ((-1, 1), (1, 0)):
            tok_co(a, df, h)

    def tok_third(a):
        tok_got(a, 2, 3)
        for h in (0, 1):
            tok_co(a, 2, h)

    def tok_partner(a):
        tok_got(a, 8, "partner")

    def chunk(dz, dx):
        return (ring(z, dz) * 4 + ring(x, dx)) * 128

    def offs(half, d1, d2):
        return (d1, d2) if half == 0 else (d2, d1)

    def way(half, second, s):
        return ("zx"[half ^ second]) + ("p" if s > 0 else "m")

    def w_piece(w, half, d1, d2):
        dz, dx = offs(half, d1, d2)
        return weights[w].at[rows(chunk(dz, dx) + half * 64, 64), :]

    def w_send(w, half, d1, d2, second, s, stage):
        p = w_piece(w, half, d1, d2)
        send(way(half, second, s), p, p, ("w", w, *stage))

    def w_got(w, pieces, stage):
        got(weights[w].at[0 : 64 * pieces, :], ("w", w, *stage))

    def w_own(w):
        for second in (0, 1):
            for half in (0, 1):
                for s in (1, -1):
                    w_send(w, half, 0, 0, second, s, (3, 0) if second else (1, s))

    def w_first(w, s):
        w_got(w, 2, (1, s))
        if s == TURN[w]:
            for half in (0, 1):
                w_send(w, half, -s, 0, 0, s, (2,))
        for half in (0, 1):
            for e in (1, -1):
                w_send(w, half, -s, 0, 1, e, (3, -s % 4))

    def w_second(w):
        w_got(w, 2, (2,))
        for half in (0, 1):
            for e in (1, -1):
                w_send(w, half, 2, 0, 1, e, (3, 2))

    def w_third(w, d1):
        w_got(w, 4, (3, d1))
        s = 1 if d1 in PLUS[w] else -1
        for half in (0, 1):
            w_send(w, half, d1, -s, 1, s, (4,))

    def w_last(w):
        w_got(w, 8, (4,))

    def unit(w, half, da, db):
        dz, dx = (db, da) if half == 0 else (da, db)
        return parts[w].at[rows(chunk(dz, dx), 128), half * 512 : half * 512 + 512]

    def rs_way(half, second, s):
        return way(1 - half, second, s)

    def sign(w, db):
        return 1 if db % 4 in PLUS[w] else -1

    def rs_got(w, units, stage):
        got(parts[w].at[0 : 128 * units, 0:512], ("rs", w, *stage))

    def end1(w, half, db, s):
        return (lft1 if s > 0 else rgt1).at[w, half, db]

    def end2(w, half, s):
        return (lft2 if s > 0 else rgt2).at[w, half]

    def far(w, half, db):
        send(rs_way(half, 0, sign(w, db)), unit(w, half, 2, db), fwd1.at[w, half, db], ("rs", w, 1, db))

    def rs_far(w, dz):
        far(w, 0, dz)
        if dz == 2:
            for db in (2, 1, 3, 0):
                far(w, 1, db)

    def rs_near(w, db):
        s = -sign(w, db)
        for half in (0, 1):
            send(rs_way(half, 0, s), unit(w, half, s, db), end1(w, half, db, s), ("rs", w, 2, db))

    def rs_relay(w, db):
        s = sign(w, db)
        rs_got(w, 2, (1, db))
        for half in (0, 1):
            mine = unit(w, half, s, db)
            add(mine, mine, fwd1.at[w, half, db])
            send(rs_way(half, 0, s), mine, end1(w, half, db, s), ("rs", w, 2, db))

    def rs_mid(w, db):
        s = TURN[w]
        rs_got(w, 4, (2, db))
        if db == s % 4:
            rs_got(w, 2, (3,))
        elif db == 0:
            rs_got(w, 4, (4,))
        for half in (0, 1):
            terms = [unit(w, half, 0, db), lft1.at[w, half, db], rgt1.at[w, half, db]]
            mine = sum1.at[w, half, db]
            if db == 2:
                add(mine, *terms)
                send(rs_way(half, 1, s), mine, fwd2.at[w, half], ("rs", w, 3))
            elif db == -s % 4:
                add(mine, *terms)
                send(rs_way(half, 1, -s), mine, end2(w, half, -s), ("rs", w, 4))
            elif db == s % 4:
                add(mine, *terms, fwd2.at[w, half])
                send(rs_way(half, 1, s), mine, end2(w, half, s), ("rs", w, 4))
            else:
                out = (gd_out, gu_out)[w].at[:, half * 512 : half * 512 + 512]
                add(out, *terms, lft2.at[w, half], rgt2.at[w, half], scale=factor)

    def block(df, mine):
        core = tp if mine else 1 - tp
        return (ring(fs, df) * 2 + core) * 128

    def gi_rows(df, h):
        return part_i.at[rows(block(df, True) + h * 64, 64), :]

    def gi_pair():
        for df in (2, 1, 3, 0):
            src = part_i.at[rows(block(df, False), 128), :]
            send("co", src, pair_in.at[df], ("gi", 0, df))

    def gi_got(pieces, stage):
        got(part_i.at[0 : 64 * pieces, :], ("gi", 0, stage))

    def gi_sum(df):
        gi_got(2, df)
        mine = part_i.at[rows(block(df, True), 128), :]
        add(mine, mine, pair_in.at[df], size=16)

    def gi_far():
        gi_sum(2)
        send("yp", gi_rows(2, 0), hop_f.at[0], ("gi", 0, "far"))
        send("ym", gi_rows(2, 1), hop_f.at[1], ("gi", 0, "far"))
        gi_sum(1)
        send("yp", gi_rows(1, 1), hop_l.at[1], ("gi", 0, "end"))
        gi_sum(3)
        send("ym", gi_rows(3, 0), hop_r.at[0], ("gi", 0, "end"))

    def gi_relay():
        gi_got(2, "far")
        add(gi_rows(1, 0), gi_rows(1, 0), hop_f.at[0], size=16)
        send("yp", gi_rows(1, 0), hop_l.at[0], ("gi", 0, "end"))
        add(gi_rows(3, 1), gi_rows(3, 1), hop_f.at[1], size=16)
        send("ym", gi_rows(3, 1), hop_r.at[1], ("gi", 0, "end"))

    def gi_end():
        gi_got(2, 0)
        gi_got(4, "end")
        for h in (0, 1):
            add(
                gi_out.at[pl.ds(h * 64, 64), :],
                gi_rows(0, h), pair_in.at[0, pl.ds(h * 64, 64), :], hop_l.at[h], hop_r.at[h], size=16,
            )

    def squares():
        def one(i, carry):
            r = rows(i * 32, 32)
            linear = jnp.maximum(pre[r, :].astype(F32), 0.0)
            sq[r, :] = (linear * linear).astype(BF16)
            return carry

        lax.fori_loop(0, 32, one, 0)

    def grad_tile(w, dz):
        right = (sq, gp)[w]
        start = ring(z, dz) * 512
        turned[...] = tokens[w][:, rows(start, 512)].T

        def one(j, carry):
            c = rows(j * 512, 512)
            parts[w][rows(start, 512), c] = jnp.dot(
                turned[...], right[:, c], preferred_element_type=F32
            ).astype(BF16)
            return carry

        lax.fori_loop(0, 2, one, 0)

    def pre_tile(i, half):
        def one(j, carry):
            r, c = rows(i * 512, 512), rows(half * 512 + j * 256, 256)
            acc = jnp.dot(tok_g[r, :], w_d[:, c], preferred_element_type=F32)
            linear = jnp.maximum(pre[r, c].astype(F32), 0.0)
            gp[r, c] = (acc * 2.0 * linear).astype(BF16)
            return carry

        lax.fori_loop(0, 2, one, 0)

    def term_tile(i, half):
        def one(j, carry):
            r, c = rows(i * 512, 512), rows(half * 1024 + j * 512, 512)
            part_i[r, c] = lax.dot_general(
                gp[r, :], w_u[c, :], (((1,), (1,)), ((), ())), preferred_element_type=F32
            ).astype(BF16)
            return carry

        lax.fori_loop(0, 2, one, 0)

    own = rows((fs * 2 + tp) * 128, 128)
    mine = rows(rep * 128, 128)
    local = [
        pltpu.make_async_copy(src, dst, local_sem.at[n])
        for n, (src, dst) in enumerate(
            (
                (wd_in, w_d.at[mine, :]),
                (og, tok_g.at[own, :]),
                (wu_in, w_u.at[mine, :]),
                (inp, tok_x.at[own, :]),
                (pre_in, pre),
            )
        )
    ]
    for copy in local:
        copy.start()
    barrier = pltpu.get_barrier_semaphore()
    for to in target.values():
        pl.semaphore_signal(barrier, inc=1, device_id=to, device_id_type=MESH)
    pl.semaphore_wait(barrier, len(target))

    def begin():
        local[0].wait()
        w_own(0)
        local[1].wait()
        tok_own(0)
        for n in (2, 3, 4):
            local[n].wait()

    def finish():
        for w in (0, 1):
            sent(weights[w].at[0:1920, :], ("w", w))
            sent(tokens[w].at[0:896, :], ("tok", w))
            sent(parts[w].at[0:1920, :], ("rs", w))
        sent(part_i.at[0:896, :], ("gi", 0))

    events = {f.__name__: f for f in (
        begin, squares, w_own, w_first, w_second, w_third, w_last, tok_own, tok_first, tok_second, tok_third, tok_partner,
        grad_tile, rs_far, rs_near, rs_relay, rs_mid, pre_tile, term_tile, gi_pair, gi_far, gi_relay, gi_end, finish,
    )}
    for n, (what, *args) in enumerate(PLAN):
        with jax.named_scope(":".join(str(v) for v in (what, *args)) + f"#n={n}"):
            events[what](*args)


def hand_over(gi_in, gu_in, gd_in, gi_out, gu_out, gd_out, sem):
    copies = [
        pltpu.make_async_copy(src, dst, sem.at[n])
        for n, (src, dst) in enumerate(((gi_in, gi_out), (gu_in, gu_out), (gd_in, gd_out)))
    ]
    for copy in copies:
        copy.start()
    for copy in copies:
        copy.wait()


def on_device(inputs, out_grad, pre_act, w_up, w_down_t):
    hbm = pl.BlockSpec(memory_space=pltpu.HBM)
    vmem = pl.BlockSpec(memory_space=pltpu.VMEM)
    outs = (
        jax.ShapeDtypeStruct((128, 2048), BF16),
        jax.ShapeDtypeStruct((128, 1024), F32),
        jax.ShapeDtypeStruct((128, 1024), F32),
    )

    def vm(*shape, kind=BF16):
        return pltpu.VMEM(shape, kind)

    results = pl.pallas_call(
        kernel,
        out_shape=outs,
        in_specs=[hbm] * 5,
        out_specs=(vmem,) * 3,
        scratch_shapes=[
            vm(1024, 2048), vm(1024, 2048), vm(2048, 1024), vm(2048, 1024),
            vm(1024, 1024), vm(1024, 1024), vm(1024, 1024), vm(512, 1024),
            vm(2048, 1024), vm(2048, 1024), vm(1024, 2048),
            vm(2, 2, 4, 128, 512), vm(2, 2, 4, 128, 512), vm(2, 2, 4, 128, 512), vm(2, 2, 4, 128, 512),
            vm(2, 2, 128, 512), vm(2, 2, 128, 512), vm(2, 2, 128, 512),
            vm(4, 128, 2048), vm(2, 64, 2048), vm(2, 64, 2048), vm(2, 64, 2048),
            pltpu.SemaphoreType.DMA((7,)), pltpu.SemaphoreType.DMA((50,)), pltpu.SemaphoreType.DMA((5,)),
        ],
        compiler_params=pltpu.CompilerParams(
            collective_id=0, has_side_effects=True, vmem_limit_bytes=54_000_000
        ),
        name="backward",
    )(*(pltpu.with_memory_space_constraint(v, pltpu.HBM) for v in (inputs, out_grad, pre_act, w_up, w_down_t)))
    return pl.pallas_call(
        hand_over,
        out_shape=outs,
        in_specs=[vmem] * 3,
        out_specs=(hbm,) * 3,
        scratch_shapes=[pltpu.SemaphoreType.DMA((3,))],
        compiler_params=pltpu.CompilerParams(vmem_limit_bytes=4_000_000),
        name="hand_over",
    )(*results)


def solution(mesh):
    rows_all = P(("rep", "fs", "tp"), None)
    tiles = P("rep", ("fs", "tp"))
    return jax.shard_map(
        on_device,
        mesh=mesh,
        in_specs=(rows_all, rows_all, tiles, tiles, tiles),
        out_specs=(rows_all, tiles, tiles),
        check_vma=False,
    )
```

time: 111 us -> 95.7 us (0.86); the launches traced: 109 us -> 95.6 us
  Pallas kernels: 104 us -> 94.9 us
  local copies, waits for them, and re-layouts: 4.62 us -> 0 us
    pallas_call x1 -> x2, Pallas kernels: 104 us -> 94.9 us  [the longest x1 93.7 us: on_device(): pl.pallas_call(kernel, out_shape=outs, in_specs=[hbm] * 5, out_specs=(vme...]
    unnamed x5 -> x0, local copies, waits for them, and re-layouts: 4.62 us -> none
where the time goes in v2:
time: 95.7 us; the launch traced here: 95.6 us
  Pallas kernels  94.9 us (99%)
    pallas_call x1, Pallas kernels, on_device(): pl.pallas_call(kernel, out_shape=outs, in_specs=[hbm] * 5, out_specs=(vme...  93.7 us

profile of v2, /device:TPU:1, one launch (start us, length us, event | category | flops | bytes accessed | tf_op | source)
XLA Modules:
  0.0 95.6 jit_solution(9468763115186687224)
XLA Ops:
  0.6 93.7 %backward.1 = (bf16[128,2048]{1,0:T(8,128)(2,1)S(1)}, f32[128,1024]{1,0:T(8,128)S(1)}, f32[128,1024]{1,0:T(8,128)S(1)}) custom-call(bf16[128,2048]{1,0:T(8,128)(2,1)} %inp.1, bf16[128,2048]{1,0:T(8,128)(2,1)} %og.1, bf16[1024,1024]{1,0:T(8,128)(2,1)} %pre_in.1, bf16[128,1024]{1,0:T(8,128)(2,1)} %wu_in.1, bf16[128,1024]{1,0:T(8,128)(2,1)} %wd_in.1), custom_call_target="tpu_custom_call" | custom-call | tf_op jit(solution)/shard_map/backward/pallas_call | solution.py:403
  94.4 1.2 %hand_over.1 = (bf16[128,2048]{1,0:T(8,128)(2,1)}, f32[128,1024]{1,0:T(8,128)}, f32[128,1024]{1,0:T(8,128)}) custom-call(bf16[128,2048]{1,0:T(8,128)(2,1)S(1)} %get-tuple-element.6.gi_in, f32[128,1024]{1,0:T(8,128)S(1)} %get-tuple-element.7.gu_in, f32[128,1024]{1,0:T(8,128)S(1)} %get-tuple-element.8.gd_in), custom_call_target="tpu_custom_call" | custom-call | tf_op jit(solution)/shard_map/hand_over/pallas_call | solution.py:422

commit v3 on v2

--- a/solution.py
+++ b/solution.py
@@ -11,22 +11,22 @@
 PLUS = ((0, 2), (1, 3))
 TURN = (1, -1)
 PLAN = (
-    ("begin",), ("squares",), ("w_own", 1), ("tok_first", 0), ("w_first", 0, 1), ("w_first", 0, -1),
-    ("w_first", 1, -1), ("tok_own", 1), ("tok_third", 0), ("w_second", 0), ("tok_second", 0), ("w_second", 1),
-    ("w_third", 0, 3), ("tok_partner", 0), ("w_third", 0, 0), ("grad_tile", 0, 2), ("w_third", 0, 1),
-    ("tok_first", 1), ("w_first", 1, 1), ("w_third", 1, 2), ("w_third", 0, 2), ("grad_tile", 0, 1),
-    ("rs_far", 0, 2), ("grad_tile", 0, 0), ("rs_near", 0, 1), ("grad_tile", 0, 3), ("rs_far", 0, 3),
-    ("w_third", 1, 0), ("w_last", 0), ("w_third", 1, 1), ("w_third", 1, 3), ("pre_tile", 1, 1),
-    ("tok_second", 1), ("pre_tile", 0, 0), ("pre_tile", 0, 1), ("rs_near", 0, 0), ("tok_third", 1),
-    ("rs_relay", 0, 2), ("tok_partner", 1), ("pre_tile", 1, 0), ("rs_near", 0, 2), ("rs_far", 0, 0),
-    ("grad_tile", 1, 2), ("rs_far", 0, 1), ("rs_far", 1, 2), ("grad_tile", 1, 1), ("grad_tile", 1, 3),
-    ("rs_relay", 0, 3), ("rs_far", 1, 1), ("rs_near", 1, 1), ("w_last", 1), ("rs_far", 1, 3),
-    ("term_tile", 0, 1), ("grad_tile", 1, 0), ("term_tile", 0, 0), ("rs_near", 0, 3), ("term_tile", 1, 1),
-    ("rs_near", 1, 0), ("rs_relay", 1, 2), ("rs_near", 1, 2), ("rs_far", 1, 0), ("term_tile", 1, 0),
-    ("rs_mid", 0, 2), ("gi_pair",), ("rs_relay", 0, 1), ("rs_relay", 1, 3), ("rs_relay", 1, 1),
-    ("rs_relay", 0, 0), ("gi_far",), ("rs_near", 1, 3), ("rs_mid", 1, 2), ("rs_mid", 0, 3), ("gi_relay",),
-    ("rs_mid", 0, 1), ("rs_relay", 1, 0), ("rs_mid", 1, 3), ("rs_mid", 1, 1), ("rs_mid", 0, 0), ("gi_end",),
-    ("rs_mid", 1, 0), ("finish",),
+    ("begin",), ("w_own", 1), ("w_first", 0, 1), ("w_first", 1, 1), ("tok_first", 0), ("squares",),
+    ("w_first", 1, -1), ("tok_second", 0), ("tok_own", 1), ("w_second", 0), ("tok_third", 0),
+    ("w_first", 0, -1), ("tok_partner", 0), ("w_second", 1), ("grad_tile", 0, 0), ("grad_tile", 0, 2),
+    ("w_third", 0, 3), ("grad_tile", 0, 1), ("w_third", 0, 0), ("w_third", 0, 2), ("grad_tile", 0, 3),
+    ("w_third", 0, 1), ("rs_near", 0, 2), ("tok_second", 1), ("rs_far", 0, 2), ("w_third", 1, 1),
+    ("tok_first", 1), ("w_third", 1, 3), ("rs_far", 0, 1), ("w_third", 1, 2), ("w_last", 0),
+    ("pre_tile", 1, 1), ("tok_third", 1), ("pre_tile", 0, 0), ("rs_far", 0, 3), ("rs_near", 0, 1),
+    ("rs_relay", 0, 2), ("pre_tile", 1, 0), ("rs_near", 0, 3), ("tok_partner", 1), ("w_third", 1, 0),
+    ("pre_tile", 0, 1), ("grad_tile", 1, 1), ("rs_far", 1, 1), ("rs_relay", 0, 1), ("grad_tile", 1, 2),
+    ("rs_far", 1, 2), ("grad_tile", 1, 3), ("grad_tile", 1, 0), ("rs_far", 1, 3), ("rs_near", 1, 3),
+    ("w_last", 1), ("term_tile", 1, 1), ("term_tile", 1, 0), ("rs_near", 0, 0), ("rs_near", 1, 2),
+    ("rs_mid", 0, 2), ("rs_far", 0, 0), ("term_tile", 0, 1), ("rs_relay", 1, 2), ("term_tile", 0, 0),
+    ("gi_pair",), ("rs_far", 1, 0), ("rs_near", 1, 1), ("rs_near", 1, 0), ("rs_relay", 1, 1),
+    ("rs_relay", 0, 3), ("rs_relay", 1, 3), ("gi_far",), ("rs_relay", 0, 0), ("rs_mid", 1, 2), ("gi_relay",),
+    ("rs_relay", 1, 0), ("rs_mid", 0, 3), ("rs_mid", 0, 1), ("rs_mid", 1, 3), ("rs_mid", 1, 1), ("gi_end",),
+    ("rs_mid", 0, 0), ("rs_mid", 1, 0), ("finish",),
 )
 
 
@@ -70,7 +70,7 @@
         remote("co", like, like, group, (group[0], *group[1:2])).wait_recv()
 
     def sent(like, kind):
-        remote("co", like, like, (), kind).wait_send()
+        remote("co", like, like, ("w", 0, 4), kind).wait_send()
 
     def rows(start, size):
         return pl.ds(pl.multiple_of(start, size), size)
@@ -104,6 +104,8 @@
         got(tokens[a].at[0 : 64 * pieces, :], ("tok", a, stage))
 
     def tok_own(a):
+        if a == 1:
+            local[3].wait()
         tok_y(a, 0, 0, 1, 1)
         tok_y(a, 0, 1, -1, 1)
         tok_y(a, 0, 1, 1, 2)
@@ -151,6 +153,8 @@
         got(weights[w].at[0 : 64 * pieces, :], ("w", w, *stage))
 
     def w_own(w):
+        if w == 1:
+            local[2].wait()
         for second in (0, 1):
             for half in (0, 1):
                 for s in (1, -1):
@@ -221,13 +225,14 @@
             add(mine, mine, fwd1.at[w, half, db])
             send(rs_way(half, 0, s), mine, end1(w, half, db, s), ("rs", w, 2, db))
 
+    def outs(w, half):
+        return (gd_out, gu_out)[w].at[:, half * 512 : half * 512 + 512]
+
     def rs_mid(w, db):
         s = TURN[w]
         rs_got(w, 4, (2, db))
         if db == s % 4:
             rs_got(w, 2, (3,))
-        elif db == 0:
-            rs_got(w, 4, (4,))
         for half in (0, 1):
             terms = [unit(w, half, 0, db), lft1.at[w, half, db], rgt1.at[w, half, db]]
             mine = sum1.at[w, half, db]
@@ -241,8 +246,11 @@
                 add(mine, *terms, fwd2.at[w, half])
                 send(rs_way(half, 1, s), mine, end2(w, half, s), ("rs", w, 4))
             else:
-                out = (gd_out, gu_out)[w].at[:, half * 512 : half * 512 + 512]
-                add(out, *terms, lft2.at[w, half], rgt2.at[w, half], scale=factor)
+                add(outs(w, half), *terms)
+        if db == 0:
+            rs_got(w, 4, (4,))
+            for half in (0, 1):
+                add(outs(w, half), outs(w, half), lft2.at[w, half], rgt2.at[w, half], scale=factor)
 
     def block(df, mine):
         core = tp if mine else 1 - tp
@@ -290,6 +298,8 @@
             )
 
     def squares():
+        local[4].wait()
+
         def one(i, carry):
             r = rows(i * 32, 32)
             linear = jnp.maximum(pre[r, :].astype(F32), 0.0)
@@ -346,7 +356,7 @@
             )
         )
     ]
-    for copy in local:
+    for copy in local[:2]:
         copy.start()
     barrier = pltpu.get_barrier_semaphore()
     for to in target.values():
@@ -358,8 +368,8 @@
         w_own(0)
         local[1].wait()
         tok_own(0)
-        for n in (2, 3, 4):
-            local[n].wait()
+        for copy in local[2:]:
+            copy.start()
 
     def finish():
         for w in (0, 1):

time: 95.7 us -> 94.6 us (0.989)
  Pallas kernels: 94.9 us -> 93.7 us
    pallas_call x1, Pallas kernels: 93.7 us -> 92.5 us  [on_device(): pl.pallas_call(kernel, out_shape=outs, in_specs=[hbm] * 5, out_specs=(vme...]
where the time goes in v3:
time: 94.6 us; the launch traced here: 94.3 us
  Pallas kernels  93.7 us (99%)
    pallas_call x1, Pallas kernels, on_device(): pl.pallas_call(kernel, out_shape=outs, in_specs=[hbm] * 5, out_specs=(vme...  92.5 us

profile of v3, /device:TPU:1, one launch (start us, length us, event | category | flops | bytes accessed | tf_op | source)
XLA Modules:
  0.0 94.3 jit_solution(5900147875710765059)
XLA Ops:
  0.6 92.5 %backward.1 = (bf16[128,2048]{1,0:T(8,128)(2,1)S(1)}, f32[128,1024]{1,0:T(8,128)S(1)}, f32[128,1024]{1,0:T(8,128)S(1)}) custom-call(bf16[128,2048]{1,0:T(8,128)(2,1)} %inp.1, bf16[128,2048]{1,0:T(8,128)(2,1)} %og.1, bf16[1024,1024]{1,0:T(8,128)(2,1)} %pre_in.1, bf16[128,1024]{1,0:T(8,128)(2,1)} %wu_in.1, bf16[128,1024]{1,0:T(8,128)(2,1)} %wd_in.1), custom_call_target="tpu_custom_call" | custom-call | tf_op jit(solution)/shard_map/backward/pallas_call | solution.py:413
  93.2 1.2 %hand_over.1 = (bf16[128,2048]{1,0:T(8,128)(2,1)}, f32[128,1024]{1,0:T(8,128)}, f32[128,1024]{1,0:T(8,128)}) custom-call(bf16[128,2048]{1,0:T(8,128)(2,1)S(1)} %get-tuple-element.6.gi_in, f32[128,1024]{1,0:T(8,128)S(1)} %get-tuple-element.7.gu_in, f32[128,1024]{1,0:T(8,128)S(1)} %get-tuple-element.8.gd_in), custom_call_target="tpu_custom_call" | custom-call | tf_op jit(solution)/shard_map/hand_over/pallas_call | solution.py:432

commit v4 on v3

--- a/solution.py
+++ b/solution.py
@@ -10,23 +10,24 @@
 STEP = {"zp": (1, 0), "zm": (-1, 0), "xp": (0, 1), "xm": (0, -1)}
 PLUS = ((0, 2), (1, 3))
 TURN = (1, -1)
+DETOUR = 16
 PLAN = (
-    ("begin",), ("w_own", 1), ("w_first", 0, 1), ("w_first", 1, 1), ("tok_first", 0), ("squares",),
-    ("w_first", 1, -1), ("tok_second", 0), ("tok_own", 1), ("w_second", 0), ("tok_third", 0),
-    ("w_first", 0, -1), ("tok_partner", 0), ("w_second", 1), ("grad_tile", 0, 0), ("grad_tile", 0, 2),
-    ("w_third", 0, 3), ("grad_tile", 0, 1), ("w_third", 0, 0), ("w_third", 0, 2), ("grad_tile", 0, 3),
-    ("w_third", 0, 1), ("rs_near", 0, 2), ("tok_second", 1), ("rs_far", 0, 2), ("w_third", 1, 1),
-    ("tok_first", 1), ("w_third", 1, 3), ("rs_far", 0, 1), ("w_third", 1, 2), ("w_last", 0),
-    ("pre_tile", 1, 1), ("tok_third", 1), ("pre_tile", 0, 0), ("rs_far", 0, 3), ("rs_near", 0, 1),
-    ("rs_relay", 0, 2), ("pre_tile", 1, 0), ("rs_near", 0, 3), ("tok_partner", 1), ("w_third", 1, 0),
-    ("pre_tile", 0, 1), ("grad_tile", 1, 1), ("rs_far", 1, 1), ("rs_relay", 0, 1), ("grad_tile", 1, 2),
-    ("rs_far", 1, 2), ("grad_tile", 1, 3), ("grad_tile", 1, 0), ("rs_far", 1, 3), ("rs_near", 1, 3),
-    ("w_last", 1), ("term_tile", 1, 1), ("term_tile", 1, 0), ("rs_near", 0, 0), ("rs_near", 1, 2),
-    ("rs_mid", 0, 2), ("rs_far", 0, 0), ("term_tile", 0, 1), ("rs_relay", 1, 2), ("term_tile", 0, 0),
-    ("gi_pair",), ("rs_far", 1, 0), ("rs_near", 1, 1), ("rs_near", 1, 0), ("rs_relay", 1, 1),
-    ("rs_relay", 0, 3), ("rs_relay", 1, 3), ("gi_far",), ("rs_relay", 0, 0), ("rs_mid", 1, 2), ("gi_relay",),
-    ("rs_relay", 1, 0), ("rs_mid", 0, 3), ("rs_mid", 0, 1), ("rs_mid", 1, 3), ("rs_mid", 1, 1), ("gi_end",),
-    ("rs_mid", 0, 0), ("rs_mid", 1, 0), ("finish",),
+    ("begin",), ("w_own", 1), ("tok_first", 0), ("w_first", 0, -1), ("w_first", 0, 1), ("w_first", 1, -1),
+    ("tok_own", 1), ("tok_second", 0), ("squares",), ("w_second", 0), ("w_third", 0, 1), ("tok_third", 0),
+    ("w_first", 1, 1), ("tok_partner", 0), ("grad_tile", 0, 2), ("tok_first", 1), ("w_third", 0, 3),
+    ("w_third", 0, 0), ("w_third", 0, 2), ("w_second", 1), ("grad_tile", 0, 3), ("w_third", 1, 0),
+    ("rs_far", 0, 2), ("grad_tile", 0, 1), ("rs_far", 0, 3), ("grad_tile", 0, 0), ("w_last", 0),
+    ("rs_near", 0, 1), ("pre_tile", 0, 1), ("w_third", 1, 1), ("w_third", 1, 2), ("rs_far", 0, 1),
+    ("pre_tile", 0, 0), ("tok_third", 1), ("pre_tile", 1, 1), ("tok_second", 1), ("w_third", 1, 3),
+    ("pre_tile", 1, 0), ("tok_partner", 1), ("rs_near", 0, 3), ("grad_tile", 1, 2), ("rs_relay", 0, 2),
+    ("rs_far", 1, 2), ("rs_near", 0, 2), ("rs_far", 0, 0), ("grad_tile", 1, 3), ("rs_far", 1, 3),
+    ("rs_relay", 0, 1), ("grad_tile", 1, 1), ("w_last", 1), ("term_tile", 1, 0), ("rs_far", 1, 1),
+    ("rs_relay", 0, 3), ("term_tile", 0, 1), ("term_tile", 1, 1), ("rs_relay", 1, 2), ("rs_near", 1, 3),
+    ("rs_mid", 0, 2), ("rs_near", 1, 2), ("term_tile", 0, 0), ("rs_near", 1, 1), ("gi_pair",),
+    ("grad_tile", 1, 0), ("rs_relay", 1, 1), ("gi_far",), ("rs_relay", 0, 0), ("rs_mid", 0, 3),
+    ("rs_far", 1, 0), ("rs_relay", 1, 3), ("rs_mid", 1, 2), ("rs_near", 0, 0), ("rs_mid", 0, 1),
+    ("rs_mid", 1, 1), ("rs_near", 1, 0), ("rs_relay", 1, 0), ("gi_relay",), ("rs_mid", 1, 3),
+    ("rs_mid", 0, 0), ("gi_end",), ("rs_mid", 1, 0), ("finish",),
 )
 
 
@@ -60,7 +61,7 @@
         n = groups.setdefault(group, len(groups))
         return pltpu.make_async_remote_copy(
             src_ref=src, dst_ref=dst, send_sem=send_sem.at[k], recv_sem=recv_sem.at[n],
-            device_id=target[to], device_id_type=MESH,
+            device_id=target[to] if isinstance(to, str) else to, device_id_type=MESH,
         )
 
     def send(to, src, dst, group):
@@ -73,7 +74,7 @@
         remote("co", like, like, ("w", 0, 4), kind).wait_send()
 
     def rows(start, size):
-        return pl.ds(pl.multiple_of(start, size), size)
+        return pl.ds(pl.multiple_of(start, size & -size), size)
 
     def add(dst, *srcs, size=32, scale=None):
         def one(i, carry):
@@ -141,9 +142,9 @@
     def way(half, second, s):
         return ("zx"[half ^ second]) + ("p" if s > 0 else "m")
 
-    def w_piece(w, half, d1, d2):
+    def w_piece(w, half, d1, d2, off=0, size=64):
         dz, dx = offs(half, d1, d2)
-        return weights[w].at[rows(chunk(dz, dx) + half * 64, 64), :]
+        return weights[w].at[rows(chunk(dz, dx) + half * 64 + off, size), :]
 
     def w_send(w, half, d1, d2, second, s, stage):
         p = w_piece(w, half, d1, d2)
@@ -175,11 +176,25 @@
             for e in (1, -1):
                 w_send(w, half, 2, 0, 1, e, (3, 2))
 
+    def w_detour(half):
+        at = (x, z)[half]
+        p = w_piece(0, half, 0, -1, 0, 64 - DETOUR)
+        send(way(half, 1, 1), p, p, ("w", 0, 4))
+        turn = 1 - 2 * lax.rem(at, 2)
+        other = lax.rem(at + turn + 4, 4)
+        back = lax.rem(at - turn + 4, 4)
+        start = (z * 4 + back if half == 0 else back * 4 + x) * 128 + half * 64 + 64 - DETOUR
+        q = w_d.at[rows(start, DETOUR), :]
+        send({"rep": z * 4 + other if half == 0 else other * 4 + x}, q, q, ("w", 0, 4))
+
     def w_third(w, d1):
         w_got(w, 4, (3, d1))
         s = 1 if d1 in PLUS[w] else -1
         for half in (0, 1):
-            w_send(w, half, d1, -s, 1, s, (4,))
+            if (w, d1) == (0, 0):
+                w_detour(half)
+            else:
+                w_send(w, half, d1, -s, 1, s, (4,))
 
     def w_last(w):
         w_got(w, 8, (4,))

time: 94.6 us -> 94 us (level)
  no operation moved by 1% of the time
where the time goes in v4:
time: 94 us; the launch traced here: 93.8 us
  Pallas kernels  93.1 us (99%)
    pallas_call x1, Pallas kernels, on_device(): pl.pallas_call(kernel, out_shape=outs, in_specs=[hbm] * 5, out_specs=(vme...  92 us

profile of v4, /device:TPU:1, one launch (start us, length us, event | category | flops | bytes accessed | tf_op | source)
XLA Modules:
  0.0 93.8 jit_solution(6611138674810382657)
XLA Ops:
  0.6 92.0 %backward.1 = (bf16[128,2048]{1,0:T(8,128)(2,1)S(1)}, f32[128,1024]{1,0:T(8,128)S(1)}, f32[128,1024]{1,0:T(8,128)S(1)}) custom-call(bf16[128,2048]{1,0:T(8,128)(2,1)} %inp.1, bf16[128,2048]{1,0:T(8,128)(2,1)} %og.1, bf16[1024,1024]{1,0:T(8,128)(2,1)} %pre_in.1, bf16[128,1024]{1,0:T(8,128)(2,1)} %wu_in.1, bf16[128,1024]{1,0:T(8,128)(2,1)} %wd_in.1), custom_call_target="tpu_custom_call" | custom-call | tf_op jit(solution)/shard_map/backward/pallas_call | solution.py:428
  92.6 1.2 %hand_over.1 = (bf16[128,2048]{1,0:T(8,128)(2,1)}, f32[128,1024]{1,0:T(8,128)}, f32[128,1024]{1,0:T(8,128)}) custom-call(bf16[128,2048]{1,0:T(8,128)(2,1)S(1)} %get-tuple-element.6.gi_in, f32[128,1024]{1,0:T(8,128)S(1)} %get-tuple-element.7.gu_in, f32[128,1024]{1,0:T(8,128)S(1)} %get-tuple-element.8.gd_in), custom_call_target="tpu_custom_call" | custom-call | tf_op jit(solution)/shard_map/hand_over/pallas_call | solution.py:447

commit v5 on v4

--- a/solution.py
+++ b/solution.py
@@ -12,22 +12,22 @@
 TURN = (1, -1)
 DETOUR = 16
 PLAN = (
-    ("begin",), ("w_own", 1), ("tok_first", 0), ("w_first", 0, -1), ("w_first", 0, 1), ("w_first", 1, -1),
-    ("tok_own", 1), ("tok_second", 0), ("squares",), ("w_second", 0), ("w_third", 0, 1), ("tok_third", 0),
-    ("w_first", 1, 1), ("tok_partner", 0), ("grad_tile", 0, 2), ("tok_first", 1), ("w_third", 0, 3),
-    ("w_third", 0, 0), ("w_third", 0, 2), ("w_second", 1), ("grad_tile", 0, 3), ("w_third", 1, 0),
-    ("rs_far", 0, 2), ("grad_tile", 0, 1), ("rs_far", 0, 3), ("grad_tile", 0, 0), ("w_last", 0),
-    ("rs_near", 0, 1), ("pre_tile", 0, 1), ("w_third", 1, 1), ("w_third", 1, 2), ("rs_far", 0, 1),
-    ("pre_tile", 0, 0), ("tok_third", 1), ("pre_tile", 1, 1), ("tok_second", 1), ("w_third", 1, 3),
-    ("pre_tile", 1, 0), ("tok_partner", 1), ("rs_near", 0, 3), ("grad_tile", 1, 2), ("rs_relay", 0, 2),
-    ("rs_far", 1, 2), ("rs_near", 0, 2), ("rs_far", 0, 0), ("grad_tile", 1, 3), ("rs_far", 1, 3),
-    ("rs_relay", 0, 1), ("grad_tile", 1, 1), ("w_last", 1), ("term_tile", 1, 0), ("rs_far", 1, 1),
-    ("rs_relay", 0, 3), ("term_tile", 0, 1), ("term_tile", 1, 1), ("rs_relay", 1, 2), ("rs_near", 1, 3),
-    ("rs_mid", 0, 2), ("rs_near", 1, 2), ("term_tile", 0, 0), ("rs_near", 1, 1), ("gi_pair",),
-    ("grad_tile", 1, 0), ("rs_relay", 1, 1), ("gi_far",), ("rs_relay", 0, 0), ("rs_mid", 0, 3),
-    ("rs_far", 1, 0), ("rs_relay", 1, 3), ("rs_mid", 1, 2), ("rs_near", 0, 0), ("rs_mid", 0, 1),
-    ("rs_mid", 1, 1), ("rs_near", 1, 0), ("rs_relay", 1, 0), ("gi_relay",), ("rs_mid", 1, 3),
-    ("rs_mid", 0, 0), ("gi_end",), ("rs_mid", 1, 0), ("finish",),
+    ("begin",), ("squares",), ("w_own", 1), ("w_first", 0, -1), ("tok_first", 0), ("w_first", 0, 1),
+    ("tok_own", 1), ("w_first", 1, -1), ("tok_second", 0), ("tok_third", 0), ("w_second", 0),
+    ("tok_partner", 0), ("w_first", 1, 1), ("w_third", 0, 1), ("w_third", 0, 0), ("w_second", 1),
+    ("grad_tile", 0, 0), ("grad_tile", 0, 3), ("grad_tile", 0, 2), ("w_third", 0, 3), ("rs_near", 0, 2),
+    ("w_third", 0, 2), ("grad_tile", 0, 1), ("rs_far", 0, 2), ("w_third", 1, 0), ("tok_second", 1),
+    ("tok_first", 1), ("rs_near", 0, 3), ("rs_far", 0, 3), ("rs_far", 0, 0), ("rs_far", 0, 1),
+    ("w_third", 1, 2), ("w_last", 0), ("tok_third", 1), ("pre_tile", 1, 1), ("w_third", 1, 3),
+    ("w_third", 1, 1), ("pre_tile", 0, 1), ("tok_partner", 1), ("pre_tile", 1, 0), ("pre_tile", 0, 0),
+    ("grad_tile", 1, 2), ("rs_relay", 0, 2), ("rs_far", 1, 2), ("grad_tile", 1, 3), ("grad_tile", 1, 1),
+    ("rs_near", 1, 3), ("rs_far", 1, 3), ("rs_relay", 0, 0), ("rs_relay", 0, 3), ("rs_far", 1, 1),
+    ("w_last", 1), ("rs_near", 1, 2), ("term_tile", 0, 1), ("term_tile", 0, 0), ("rs_relay", 1, 2),
+    ("term_tile", 1, 1), ("rs_mid", 0, 2), ("rs_relay", 0, 1), ("term_tile", 1, 0), ("gi_pair",),
+    ("rs_near", 1, 1), ("rs_near", 0, 1), ("gi_far",), ("rs_relay", 1, 1), ("rs_relay", 1, 3),
+    ("grad_tile", 1, 0), ("rs_far", 1, 0), ("rs_mid", 1, 2), ("rs_near", 0, 0), ("rs_mid", 0, 3),
+    ("rs_near", 1, 0), ("rs_relay", 1, 0), ("gi_relay",), ("rs_mid", 0, 1), ("rs_mid", 1, 1),
+    ("rs_mid", 1, 3), ("gi_end",), ("rs_mid", 0, 0), ("rs_mid", 1, 0), ("finish",),
 )
 
 
@@ -35,7 +35,7 @@
     inp, og, pre_in, wu_in, wd_in, gi_out, gu_out, gd_out,
     tok_g, tok_x, w_d, w_u, pre, sq, gp, turned, part_d, part_u, part_i,
     fwd1, lft1, rgt1, sum1, fwd2, lft2, rgt2,
-    pair_in, hop_f, hop_l, hop_r, send_sem, recv_sem, local_sem,
+    pair_in, hop_f, hop_l, hop_r, send_sem, recv_sem, local_sem, ready_sem,
 ):
     rep, fs, tp = lax.axis_index("rep"), lax.axis_index("fs"), lax.axis_index("tp")
     z, x = lax.div(rep, 4), lax.rem(rep, 4)
@@ -160,6 +160,12 @@
             for half in (0, 1):
                 for s in (1, -1):
                     w_send(w, half, 0, 0, second, s, (3, 0) if second else (1, s))
+
+    def w_own_along(axis):
+        for second in (0, 1):
+            half = second if axis == "z" else 1 - second
+            for s in (1, -1):
+                w_send(0, half, 0, 0, second, s, (3, 0) if second else (1, s))
 
     def w_first(w, s):
         w_got(w, 2, (1, s))
@@ -374,15 +380,36 @@
     for copy in local[:2]:
         copy.start()
     barrier = pltpu.get_barrier_semaphore()
-    for to in target.values():
+    for name, to in target.items():
+        to = to if name == "co" else {**to, "tp": 0 if name[0] == "z" else 1}
         pl.semaphore_signal(barrier, inc=1, device_id=to, device_id_type=MESH)
-    pl.semaphore_wait(barrier, len(target))
+
+    def gather():
+        pl.semaphore_wait(barrier, 5 + 4 * tp)
+        pl.semaphore_signal(ready_sem, inc=1, device_id=target["co"], device_id_type=MESH)
+
+    def hear():
+        pl.semaphore_wait(ready_sem, 1)
+
+    def along_z():
+        w_own_along("z")
+
+    def along_xy():
+        w_own_along("x")
+        tok_own(0)
 
     def begin():
         local[0].wait()
-        w_own(0)
         local[1].wait()
-        tok_own(0)
+        later = lax.div(z + 3, 4)
+        pl.when(tp + later == 1)(gather)
+        pl.when(tp + later != 1)(hear)
+        pl.when(later == 1)(along_z)
+        pl.when(later == 0)(along_xy)
+        pl.when(tp + later == 1)(hear)
+        pl.when(tp + later != 1)(gather)
+        pl.when(later == 1)(along_xy)
+        pl.when(later == 0)(along_z)
         for copy in local[2:]:
             copy.start()
 
@@ -438,6 +465,7 @@
             vm(2, 2, 128, 512), vm(2, 2, 128, 512), vm(2, 2, 128, 512),
             vm(4, 128, 2048), vm(2, 64, 2048), vm(2, 64, 2048), vm(2, 64, 2048),
             pltpu.SemaphoreType.DMA((7,)), pltpu.SemaphoreType.DMA((50,)), pltpu.SemaphoreType.DMA((5,)),
+            pltpu.SemaphoreType.REGULAR,
         ],
         compiler_params=pltpu.CompilerParams(
             collective_id=0, has_side_effects=True, vmem_limit_bytes=54_000_000

time: 94 us -> 93.9 us (level)
  no operation moved by 1% of the time
where the time goes in v5:
time: 93.9 us; the launch traced here: 93.7 us
  Pallas kernels  93.1 us (99%)
    pallas_call x1, Pallas kernels, on_device(): pl.pallas_call(kernel, out_shape=outs, in_specs=[hbm] * 5, out_specs=(vme...  91.9 us

profile of v5, /device:TPU:1, one launch (start us, length us, event | category | flops | bytes accessed | tf_op | source)
XLA Modules:
  0.0 93.7 jit_solution(4155836792606862742)
XLA Ops:
  0.6 91.9 %backward.1 = (bf16[128,2048]{1,0:T(8,128)(2,1)S(1)}, f32[128,1024]{1,0:T(8,128)S(1)}, f32[128,1024]{1,0:T(8,128)S(1)}) custom-call(bf16[128,2048]{1,0:T(8,128)(2,1)} %inp.1, bf16[128,2048]{1,0:T(8,128)(2,1)} %og.1, bf16[1024,1024]{1,0:T(8,128)(2,1)} %pre_in.1, bf16[128,1024]{1,0:T(8,128)(2,1)} %wu_in.1, bf16[128,1024]{1,0:T(8,128)(2,1)} %wd_in.1), custom_call_target="tpu_custom_call" | custom-call | tf_op jit(solution)/shard_map/backward/pallas_call | solution.py:455
  92.5 1.2 %hand_over.1 = (bf16[128,2048]{1,0:T(8,128)(2,1)}, f32[128,1024]{1,0:T(8,128)}, f32[128,1024]{1,0:T(8,128)}) custom-call(bf16[128,2048]{1,0:T(8,128)(2,1)S(1)} %get-tuple-element.6.gi_in, f32[128,1024]{1,0:T(8,128)S(1)} %get-tuple-element.7.gu_in, f32[128,1024]{1,0:T(8,128)S(1)} %get-tuple-element.8.gd_in), custom_call_target="tpu_custom_call" | custom-call | tf_op jit(solution)/shard_map/hand_over/pallas_call | solution.py:475

commit v6 on v5

--- a/solution.py
+++ b/solution.py
@@ -33,13 +33,14 @@
 
 def kernel(
     inp, og, pre_in, wu_in, wd_in, gi_out, gu_out, gd_out,
-    tok_g, tok_x, w_d, w_u, pre, sq, gp, turned, part_d, part_u, part_i,
+    toks, mats, pre, sq, gp, turned, sums, part_i,
     fwd1, lft1, rgt1, sum1, fwd2, lft2, rgt2,
     pair_in, hop_f, hop_l, hop_r, send_sem, recv_sem, local_sem, ready_sem,
 ):
     rep, fs, tp = lax.axis_index("rep"), lax.axis_index("fs"), lax.axis_index("tp")
     z, x = lax.div(rep, 4), lax.rem(rep, 4)
-    tokens, weights, parts = (tok_g, tok_x), (w_d, w_u), (part_d, part_u)
+    tokens, weights, parts = [[ref.at[0], ref.at[1]] for ref in (toks, mats, sums)]
+    (tok_g, tok_x), (w_d, w_u) = tokens, weights
     factor = 1.0 / 128.0
 
     def ring(v, d):
@@ -65,10 +66,14 @@
         )
 
     def send(to, src, dst, group):
-        remote(to, src, dst, group, (group[0], *group[1:2])).start()
+        remote(to, src, dst, group, group[0]).start()
 
     def got(like, group):
-        remote("co", like, like, group, (group[0], *group[1:2])).wait_recv()
+        remote("co", like, like, group, group[0]).wait_recv()
+
+    def here(count, n):
+        like = w_u.at[0:count, :]
+        pltpu.make_async_copy(like, like, local_sem.at[n]).wait()
 
     def sent(like, kind):
         remote("co", like, like, ("w", 0, 4), kind).wait_send()
@@ -105,8 +110,6 @@
         got(tokens[a].at[0 : 64 * pieces, :], ("tok", a, stage))
 
     def tok_own(a):
-        if a == 1:
-            local[3].wait()
         tok_y(a, 0, 0, 1, 1)
         tok_y(a, 0, 1, -1, 1)
         tok_y(a, 0, 1, 1, 2)
@@ -154,8 +157,6 @@
         got(weights[w].at[0 : 64 * pieces, :], ("w", w, *stage))
 
     def w_own(w):
-        if w == 1:
-            local[2].wait()
         for second in (0, 1):
             for half in (0, 1):
                 for s in (1, -1):
@@ -251,15 +252,13 @@
 
     def rs_mid(w, db):
         s = TURN[w]
-        rs_got(w, 4, (2, db))
-        if db == s % 4:
-            rs_got(w, 2, (3,))
+        rs_got(w, 6 if db == s % 4 else 4, (2, db))
         for half in (0, 1):
             terms = [unit(w, half, 0, db), lft1.at[w, half, db], rgt1.at[w, half, db]]
             mine = sum1.at[w, half, db]
             if db == 2:
                 add(mine, *terms)
-                send(rs_way(half, 1, s), mine, fwd2.at[w, half], ("rs", w, 3))
+                send(rs_way(half, 1, s), mine, fwd2.at[w, half], ("rs", w, 2, s % 4))
             elif db == -s % 4:
                 add(mine, *terms)
                 send(rs_way(half, 1, -s), mine, end2(w, half, -s), ("rs", w, 4))
@@ -283,17 +282,17 @@
     def gi_pair():
         for df in (2, 1, 3, 0):
             src = part_i.at[rows(block(df, False), 128), :]
-            send("co", src, pair_in.at[df], ("gi", 0, df))
+            send("co", src, pair_in.at[df], ("gi", 0, "pair"))
 
     def gi_got(pieces, stage):
         got(part_i.at[0 : 64 * pieces, :], ("gi", 0, stage))
 
     def gi_sum(df):
-        gi_got(2, df)
         mine = part_i.at[rows(block(df, True), 128), :]
         add(mine, mine, pair_in.at[df], size=16)
 
     def gi_far():
+        gi_got(8, "pair")
         gi_sum(2)
         send("yp", gi_rows(2, 0), hop_f.at[0], ("gi", 0, "far"))
         send("ym", gi_rows(2, 1), hop_f.at[1], ("gi", 0, "far"))
@@ -310,7 +309,6 @@
         send("ym", gi_rows(3, 1), hop_r.at[1], ("gi", 0, "end"))
 
     def gi_end():
-        gi_got(2, 0)
         gi_got(4, "end")
         for h in (0, 1):
             add(
@@ -319,7 +317,7 @@
             )
 
     def squares():
-        local[4].wait()
+        here(1408, 1)
 
         def one(i, carry):
             r = rows(i * 32, 32)
@@ -366,7 +364,7 @@
     own = rows((fs * 2 + tp) * 128, 128)
     mine = rows(rep * 128, 128)
     local = [
-        pltpu.make_async_copy(src, dst, local_sem.at[n])
+        pltpu.make_async_copy(src, dst, local_sem.at[n // 2 if n < 4 else 1])
         for n, (src, dst) in enumerate(
             (
                 (wd_in, w_d.at[mine, :]),
@@ -399,8 +397,7 @@
         tok_own(0)
 
     def begin():
-        local[0].wait()
-        local[1].wait()
+        here(384, 0)
         later = lax.div(z + 3, 4)
         pl.when(tp + later == 1)(gather)
         pl.when(tp + later != 1)(hear)
@@ -414,11 +411,10 @@
             copy.start()
 
     def finish():
-        for w in (0, 1):
-            sent(weights[w].at[0:1920, :], ("w", w))
-            sent(tokens[w].at[0:896, :], ("tok", w))
-            sent(parts[w].at[0:1920, :], ("rs", w))
-        sent(part_i.at[0:896, :], ("gi", 0))
+        sent(mats.at[:, 0:1920, :], "w")
+        sent(toks.at[:, 0:896, :], "tok")
+        sent(sums.at[:, 0:1920, :], "rs")
+        sent(part_i.at[0:896, :], "gi")
 
     events = {f.__name__: f for f in (
         begin, squares, w_own, w_first, w_second, w_third, w_last, tok_own, tok_first, tok_second, tok_third, tok_partner,
@@ -458,13 +454,13 @@
         in_specs=[hbm] * 5,
         out_specs=(vmem,) * 3,
         scratch_shapes=[
-            vm(1024, 2048), vm(1024, 2048), vm(2048, 1024), vm(2048, 1024),
+            vm(2, 1024, 2048), vm(2, 2048, 1024),
             vm(1024, 1024), vm(1024, 1024), vm(1024, 1024), vm(512, 1024),
-            vm(2048, 1024), vm(2048, 1024), vm(1024, 2048),
+            vm(2, 2048, 1024), vm(1024, 2048),
             vm(2, 2, 4, 128, 512), vm(2, 2, 4, 128, 512), vm(2, 2, 4, 128, 512), vm(2, 2, 4, 128, 512),
             vm(2, 2, 128, 512), vm(2, 2, 128, 512), vm(2, 2, 128, 512),
             vm(4, 128, 2048), vm(2, 64, 2048), vm(2, 64, 2048), vm(2, 64, 2048),
-            pltpu.SemaphoreType.DMA((7,)), pltpu.SemaphoreType.DMA((50,)), pltpu.SemaphoreType.DMA((5,)),
+            pltpu.SemaphoreType.DMA((4,)), pltpu.SemaphoreType.DMA((45,)), pltpu.SemaphoreType.DMA((2,)),
             pltpu.SemaphoreType.REGULAR,
         ],
         compiler_params=pltpu.CompilerParams(

time: 93.9 us -> 93.8 us (level)
  no operation moved by 1% of the time
where the time goes in v6:
time: 93.8 us; the launch traced here: 93.6 us
  Pallas kernels  93 us (99%)
    pallas_call x1, Pallas kernels, on_device(): pl.pallas_call(kernel, out_shape=outs, in_specs=[hbm] * 5, out_specs=(vme...  91.8 us

profile of v6, /device:TPU:1, one launch (start us, length us, event | category | flops | bytes accessed | tf_op | source)
XLA Modules:
  0.0 93.6 jit_solution(2261104731531185769)
XLA Ops:
  0.6 91.8 %backward.1 = (bf16[128,2048]{1,0:T(8,128)(2,1)S(1)}, f32[128,1024]{1,0:T(8,128)S(1)}, f32[128,1024]{1,0:T(8,128)S(1)}) custom-call(bf16[128,2048]{1,0:T(8,128)(2,1)} %inp.1, bf16[128,2048]{1,0:T(8,128)(2,1)} %og.1, bf16[1024,1024]{1,0:T(8,128)(2,1)} %pre_in.1, bf16[128,1024]{1,0:T(8,128)(2,1)} %wu_in.1, bf16[128,1024]{1,0:T(8,128)(2,1)} %wd_in.1), custom_call_target="tpu_custom_call" | custom-call | tf_op jit(solution)/shard_map/backward/pallas_call | solution.py:451
  92.4 1.2 %hand_over.1 = (bf16[128,2048]{1,0:T(8,128)(2,1)}, f32[128,1024]{1,0:T(8,128)}, f32[128,1024]{1,0:T(8,128)}) custom-call(bf16[128,2048]{1,0:T(8,128)(2,1)S(1)} %get-tuple-element.6.gi_in, f32[128,1024]{1,0:T(8,128)S(1)} %get-tuple-element.7.gu_in, f32[128,1024]{1,0:T(8,128)S(1)} %get-tuple-element.8.gd_in), custom_call_target="tpu_custom_call" | custom-call | tf_op jit(solution)/shard_map/hand_over/pallas_call | solution.py:471

commit v7 on v6

--- a/solution.py
+++ b/solution.py
@@ -11,6 +11,7 @@
 PLUS = ((0, 2), (1, 3))
 TURN = (1, -1)
 DETOUR = 16
+FACTOR = 1.0 / 128.0
 PLAN = (
     ("begin",), ("squares",), ("w_own", 1), ("w_first", 0, -1), ("tok_first", 0), ("w_first", 0, 1),
     ("tok_own", 1), ("w_first", 1, -1), ("tok_second", 0), ("tok_third", 0), ("w_second", 0),
@@ -32,7 +33,7 @@
 
 
 def kernel(
-    inp, og, pre_in, wu_in, wd_in, gi_out, gu_out, gd_out,
+    inp, og, pre_in, wu_in, wd_in, gi_out, gu_out, gd_out, lft_out, rgt_out,
     toks, mats, pre, sq, gp, turned, sums, part_i,
     fwd1, lft1, rgt1, sum1, fwd2, lft2, rgt2,
     pair_in, hop_f, hop_l, hop_r, send_sem, recv_sem, local_sem, ready_sem,
@@ -41,7 +42,7 @@
     z, x = lax.div(rep, 4), lax.rem(rep, 4)
     tokens, weights, parts = [[ref.at[0], ref.at[1]] for ref in (toks, mats, sums)]
     (tok_g, tok_x), (w_d, w_u) = tokens, weights
-    factor = 1.0 / 128.0
+    factor = FACTOR
 
     def ring(v, d):
         return lax.rem(v + d % 4, 4)
@@ -223,7 +224,9 @@
         return (lft1 if s > 0 else rgt1).at[w, half, db]
 
     def end2(w, half, s):
-        return (lft2 if s > 0 else rgt2).at[w, half]
+        if w == 1:
+            return (lft_out if s > 0 else rgt_out).at[half]
+        return (lft2 if s > 0 else rgt2).at[half]
 
     def far(w, half, db):
         send(rs_way(half, 0, sign(w, db)), unit(w, half, 2, db), fwd1.at[w, half, db], ("rs", w, 1, db))
@@ -270,7 +273,8 @@
         if db == 0:
             rs_got(w, 4, (4,))
             for half in (0, 1):
-                add(outs(w, half), outs(w, half), lft2.at[w, half], rgt2.at[w, half], scale=factor)
+                if w == 0:
+                    add(outs(w, half), outs(w, half), lft2.at[half], rgt2.at[half], scale=factor)
 
     def block(df, mine):
         core = tp if mine else 1 - tp
@@ -425,13 +429,27 @@
             events[what](*args)
 
 
-def hand_over(gi_in, gu_in, gd_in, gi_out, gu_out, gd_out, sem):
+def hand_over(gi_in, gu_in, gd_in, lft_in, rgt_in, gi_out, gu_out, gd_out, done, sem):
     copies = [
         pltpu.make_async_copy(src, dst, sem.at[n])
-        for n, (src, dst) in enumerate(((gi_in, gi_out), (gu_in, gu_out), (gd_in, gd_out)))
+        for n, (src, dst) in enumerate(((gi_in, gi_out), (gd_in, gd_out)))
     ]
     for copy in copies:
         copy.start()
+    for part in (0, 1):
+
+        def one(i, carry, part=part):
+            r = pl.ds(pl.multiple_of(part * 64 + i * 16, 16), 16)
+            for half in (0, 1):
+                c = slice(half * 512, half * 512 + 512)
+                total = gu_in[r, c] + lft_in[half, r, :].astype(F32) + rgt_in[half, r, :].astype(F32)
+                done[r, c] = total * FACTOR
+            return carry
+
+        lax.fori_loop(0, 4, one, 0)
+        r = pl.ds(part * 64, 64)
+        copies.append(pltpu.make_async_copy(done.at[r, :], gu_out.at[r, :], sem.at[2 + part]))
+        copies[-1].start()
     for copy in copies:
         copy.wait()
 
@@ -450,15 +468,15 @@
 
     results = pl.pallas_call(
         kernel,
-        out_shape=outs,
+        out_shape=(*outs, *[jax.ShapeDtypeStruct((2, 128, 512), BF16)] * 2),
         in_specs=[hbm] * 5,
-        out_specs=(vmem,) * 3,
+        out_specs=(vmem,) * 5,
         scratch_shapes=[
             vm(2, 1024, 2048), vm(2, 2048, 1024),
             vm(1024, 1024), vm(1024, 1024), vm(1024, 1024), vm(512, 1024),
             vm(2, 2048, 1024), vm(1024, 2048),
             vm(2, 2, 4, 128, 512), vm(2, 2, 4, 128, 512), vm(2, 2, 4, 128, 512), vm(2, 2, 4, 128, 512),
-            vm(2, 2, 128, 512), vm(2, 2, 128, 512), vm(2, 2, 128, 512),
+            vm(2, 2, 128, 512), vm(2, 128, 512), vm(2, 128, 512),
             vm(4, 128, 2048), vm(2, 64, 2048), vm(2, 64, 2048), vm(2, 64, 2048),
             pltpu.SemaphoreType.DMA((4,)), pltpu.SemaphoreType.DMA((45,)), pltpu.SemaphoreType.DMA((2,)),
             pltpu.SemaphoreType.REGULAR,
@@ -471,9 +489,9 @@
     return pl.pallas_call(
         hand_over,
         out_shape=outs,
-        in_specs=[vmem] * 3,
+        in_specs=[vmem] * 5,
         out_specs=(hbm,) * 3,
-        scratch_shapes=[pltpu.SemaphoreType.DMA((3,))],
+        scratch_shapes=[vm(128, 1024, kind=F32), pltpu.SemaphoreType.DMA((4,))],
         compiler_params=pltpu.CompilerParams(vmem_limit_bytes=4_000_000),
         name="hand_over",
     )(*results)

time: 93.8 us -> 93.6 us (level)
  no operation moved by 1% of the time
where the time goes in v7:
time: 93.6 us; the launch traced here: 93.5 us
  Pallas kernels  92.8 us (99%)
    pallas_call x1, Pallas kernels, on_device(): pl.pallas_call(kernel, out_shape=(*outs, *[jax.ShapeDtypeStruct((2, 128,...  91.7 us

profile of v7, /device:TPU:1, one launch (start us, length us, event | category | flops | bytes accessed | tf_op | source)
XLA Modules:
  0.0 93.5 jit_solution(18405602478762994276)
XLA Ops:
  0.6 91.7 %backward.1 = (bf16[128,2048]{1,0:T(8,128)(2,1)S(1)}, f32[128,1024]{1,0:T(8,128)S(1)}, f32[128,1024]{1,0:T(8,128)S(1)}, bf16[2,128,512]{2,1,0:T(8,128)(2,1)S(1)}, bf16[2,128,512]{2,1,0:T(8,128)(2,1)S(1)}) custom-call(bf16[128,2048]{1,0:T(8,128)(2,1)} %inp.1, bf16[128,2048]{1,0:T(8,128)(2,1)} %og.1, bf16[1024,1024]{1,0:T(8,128)(2,1)} %pre_in.1, ...), custom_call_target="tpu_custom_call" | custom-call | tf_op jit(solution)/shard_map/backward/pallas_call | solution.py:469
  92.3 1.2 %hand_over.1 = (bf16[128,2048]{1,0:T(8,128)(2,1)}, f32[128,1024]{1,0:T(8,128)}, f32[128,1024]{1,0:T(8,128)}) custom-call(bf16[128,2048]{1,0:T(8,128)(2,1)S(1)} %get-tuple-element.8.gi_in, f32[128,1024]{1,0:T(8,128)S(1)} %get-tuple-element.9.gu_in, f32[128,1024]{1,0:T(8,128)S(1)} %get-tuple-element.10.gd_in, ...), custom_call_target="tpu_custom_call" | custom-call | tf_op jit(solution)/shard_map/hand_over/pallas_call | solution.py:489

commit v8 on v7

--- a/solution.py
+++ b/solution.py
@@ -13,22 +13,22 @@
 DETOUR = 16
 FACTOR = 1.0 / 128.0
 PLAN = (
-    ("begin",), ("squares",), ("w_own", 1), ("w_first", 0, -1), ("tok_first", 0), ("w_first", 0, 1),
-    ("tok_own", 1), ("w_first", 1, -1), ("tok_second", 0), ("tok_third", 0), ("w_second", 0),
-    ("tok_partner", 0), ("w_first", 1, 1), ("w_third", 0, 1), ("w_third", 0, 0), ("w_second", 1),
-    ("grad_tile", 0, 0), ("grad_tile", 0, 3), ("grad_tile", 0, 2), ("w_third", 0, 3), ("rs_near", 0, 2),
-    ("w_third", 0, 2), ("grad_tile", 0, 1), ("rs_far", 0, 2), ("w_third", 1, 0), ("tok_second", 1),
-    ("tok_first", 1), ("rs_near", 0, 3), ("rs_far", 0, 3), ("rs_far", 0, 0), ("rs_far", 0, 1),
-    ("w_third", 1, 2), ("w_last", 0), ("tok_third", 1), ("pre_tile", 1, 1), ("w_third", 1, 3),
-    ("w_third", 1, 1), ("pre_tile", 0, 1), ("tok_partner", 1), ("pre_tile", 1, 0), ("pre_tile", 0, 0),
-    ("grad_tile", 1, 2), ("rs_relay", 0, 2), ("rs_far", 1, 2), ("grad_tile", 1, 3), ("grad_tile", 1, 1),
-    ("rs_near", 1, 3), ("rs_far", 1, 3), ("rs_relay", 0, 0), ("rs_relay", 0, 3), ("rs_far", 1, 1),
-    ("w_last", 1), ("rs_near", 1, 2), ("term_tile", 0, 1), ("term_tile", 0, 0), ("rs_relay", 1, 2),
-    ("term_tile", 1, 1), ("rs_mid", 0, 2), ("rs_relay", 0, 1), ("term_tile", 1, 0), ("gi_pair",),
-    ("rs_near", 1, 1), ("rs_near", 0, 1), ("gi_far",), ("rs_relay", 1, 1), ("rs_relay", 1, 3),
-    ("grad_tile", 1, 0), ("rs_far", 1, 0), ("rs_mid", 1, 2), ("rs_near", 0, 0), ("rs_mid", 0, 3),
-    ("rs_near", 1, 0), ("rs_relay", 1, 0), ("gi_relay",), ("rs_mid", 0, 1), ("rs_mid", 1, 1),
-    ("rs_mid", 1, 3), ("gi_end",), ("rs_mid", 0, 0), ("rs_mid", 1, 0), ("finish",),
+    ("begin",), ("squares",), ("w_own", 1), ("w_first", 0, 1), ("w_first", 1, -1), ("w_first", 0, -1),
+    ("tok_first", 0), ("w_second", 0), ("tok_own", 1), ("tok_third", 0), ("tok_second", 0), ("w_first", 1, 1),
+    ("w_third", 0, 0), ("tok_partner", 0), ("w_second", 1), ("grad_tile", 0, 2), ("grad_tile", 0, 0),
+    ("grad_tile", 0, 1), ("w_third", 0, 3), ("w_third", 0, 1), ("w_third", 0, 2), ("rs_far", 0, 2),
+    ("tok_first", 1), ("grad_tile", 0, 3), ("w_third", 1, 1), ("w_third", 1, 0), ("w_third", 1, 2),
+    ("w_last", 0), ("rs_far", 0, 3), ("w_third", 1, 3), ("tok_third", 1), ("rs_near", 0, 3),
+    ("rs_near", 0, 1), ("pre_tile", 1, 0), ("rs_relay", 0, 2), ("rs_near", 0, 2), ("rs_far", 0, 1),
+    ("tok_second", 1), ("pre_tile", 0, 1), ("tok_partner", 1), ("pre_tile", 0, 0), ("pre_tile", 1, 1),
+    ("rs_relay", 0, 3), ("grad_tile", 1, 2), ("rs_far", 0, 0), ("grad_tile", 1, 1), ("rs_far", 1, 2),
+    ("grad_tile", 1, 3), ("rs_relay", 0, 1), ("rs_far", 1, 3), ("rs_far", 1, 1), ("rs_near", 1, 3),
+    ("rs_near", 1, 2), ("w_last", 1), ("term_tile", 1, 1), ("term_tile", 0, 0), ("term_tile", 1, 0),
+    ("term_tile", 0, 1), ("rs_mid", 0, 2), ("rs_relay", 1, 2), ("gi_pair",), ("rs_near", 0, 0),
+    ("rs_relay", 0, 0), ("rs_relay", 1, 1), ("gi_far",), ("rs_near", 1, 1), ("grad_tile", 1, 0),
+    ("rs_far", 1, 0), ("rs_mid", 1, 2), ("rs_relay", 1, 3), ("rs_mid", 0, 1), ("rs_near", 1, 0),
+    ("gi_relay",), ("rs_mid", 0, 3), ("rs_mid", 1, 1), ("rs_relay", 1, 0), ("rs_mid", 1, 3), ("rs_mid", 0, 0),
+    ("gi_end",), ("rs_mid", 1, 0), ("finish",),
 )
 
 
@@ -381,13 +381,14 @@
     ]
     for copy in local[:2]:
         copy.start()
+    later = lax.div(z + 3, 4)
     barrier = pltpu.get_barrier_semaphore()
     for name, to in target.items():
-        to = to if name == "co" else {**to, "tp": 0 if name[0] == "z" else 1}
+        to = to if name == "co" else {**to, "tp": {"z": 0, "x": 1, "y": later}[name[0]]}
         pl.semaphore_signal(barrier, inc=1, device_id=to, device_id_type=MESH)
 
     def gather():
-        pl.semaphore_wait(barrier, 5 + 4 * tp)
+        pl.semaphore_wait(barrier, 9 - 4 * (tp - later) * (tp - later))
         pl.semaphore_signal(ready_sem, inc=1, device_id=target["co"], device_id_type=MESH)
 
     def hear():
@@ -396,21 +397,20 @@
     def along_z():
         w_own_along("z")
 
-    def along_xy():
+    def along_x():
         w_own_along("x")
-        tok_own(0)
 
     def begin():
         here(384, 0)
-        later = lax.div(z + 3, 4)
         pl.when(tp + later == 1)(gather)
         pl.when(tp + later != 1)(hear)
         pl.when(later == 1)(along_z)
-        pl.when(later == 0)(along_xy)
+        pl.when(later == 0)(along_x)
         pl.when(tp + later == 1)(hear)
         pl.when(tp + later != 1)(gather)
-        pl.when(later == 1)(along_xy)
+        pl.when(later == 1)(along_x)
         pl.when(later == 0)(along_z)
+        tok_own(0)
         for copy in local[2:]:
             copy.start()
 

time: 93.6 us -> 93.6 us (level)
  no operation moved by 1% of the time
where the time goes in v8:
time: 93.6 us; the launch traced here: 93.5 us
  Pallas kernels  92.8 us (99%)
    pallas_call x1, Pallas kernels, on_device(): pl.pallas_call(kernel, out_shape=(*outs, *[jax.ShapeDtypeStruct((2, 128,...  91.6 us

profile of v8, /device:TPU:1, one launch (start us, length us, event | category | flops | bytes accessed | tf_op | source)
XLA Modules:
  0.0 93.5 jit_solution(3054358471590349056)
XLA Ops:
  0.6 91.6 %backward.1 = (bf16[128,2048]{1,0:T(8,128)(2,1)S(1)}, f32[128,1024]{1,0:T(8,128)S(1)}, f32[128,1024]{1,0:T(8,128)S(1)}, bf16[2,128,512]{2,1,0:T(8,128)(2,1)S(1)}, bf16[2,128,512]{2,1,0:T(8,128)(2,1)S(1)}) custom-call(bf16[128,2048]{1,0:T(8,128)(2,1)} %inp.1, bf16[128,2048]{1,0:T(8,128)(2,1)} %og.1, bf16[1024,1024]{1,0:T(8,128)(2,1)} %pre_in.1, ...), custom_call_target="tpu_custom_call" | custom-call | tf_op jit(solution)/shard_map/backward/pallas_call | solution.py:469
  92.3 1.2 %hand_over.1 = (bf16[128,2048]{1,0:T(8,128)(2,1)}, f32[128,1024]{1,0:T(8,128)}, f32[128,1024]{1,0:T(8,128)}) custom-call(bf16[128,2048]{1,0:T(8,128)(2,1)S(1)} %get-tuple-element.8.gi_in, f32[128,1024]{1,0:T(8,128)S(1)} %get-tuple-element.9.gu_in, f32[128,1024]{1,0:T(8,128)S(1)} %get-tuple-element.10.gd_in, ...), custom_call_target="tpu_custom_call" | custom-call | tf_op jit(solution)/shard_map/hand_over/pallas_call | solution.py:489
